TPU v7x, 256 devices: a whole 4x4x8 slice. The times are simulated.
256 devices in a mesh: sp: 32 (over z, x), tp: 8 (over y, core).
Axes of the slice: x: 4, y: 4, z: 8, core: 2. Of those that a mesh axis runs over, the one named last changes fastest.
Arguments:
- upstream: bfloat16 [8192, 2048], P('sp'), may hold values from -6 to 6
- stream: bfloat16 [8192, 2048], P('sp'), may hold values from -10 to 10
- routes: int32 [8192, 2], P('sp'), may hold values from 0 to 31, all different within a row; in each aligned block of 256 rows (0 to 255, 256 to 511, ...) at most 32 rows name the same one
- route_weights: float32 [8192, 2], P('sp'), may hold values from 0.1 to 1
- glu_value: bfloat16 [8192, 512], P('sp', 'tp'), may hold values from -6 to 6
- glu_gate: bfloat16 [8192, 512], P('sp', 'tp'), may hold values from -10 to 10
- conv_taps: float32 [31, 512], P(None, 'tp'), may hold values from -1 to 1
- conv_saved: bfloat16 [8192, 512], P('sp', 'tp'), may hold values from -600 to 600
- out_proj: bfloat16 [2048, 512], P(None, 'tp'), may hold values from -0.25 to 0.25
- expert_gate: bfloat16 [32, 2048, 2048], P('sp', None, 'tp'), may hold values from -0.125 to 0.125
- expert_up: bfloat16 [32, 2048, 2048], P('sp', None, 'tp'), may hold values from -0.125 to 0.125
- expert_down: bfloat16 [32, 2048, 2048], P('sp', 'tp'), may hold values from -0.125 to 0.125
Outputs:
- grad_stream: bfloat16 [8192, 2048], P('sp', 'tp')
- grad_value: bfloat16 [8192, 512], P('sp', 'tp')
- grad_gate: bfloat16 [8192, 512], P('sp', 'tp')
- grad_out_proj: float32 [2048, 512], P('sp', 'tp')
- grad_expert_gate: float32 [32, 2048, 2048], P('sp', None, 'tp')
- grad_expert_up: float32 [32, 2048, 2048], P('sp', None, 'tp')
- grad_expert_down: float32 [32, 2048, 2048], P('sp', 'tp')
Inputs may be any that keep to these rules, and one draw needn't show every extreme that they name: `routes`: each row names 2 different experts; among the 256 rows of one index of sp no expert is named more than 32 times, a bound that some block reaches.
All inputs are finite; a program needn't handle non-finite values.
Results may differ from a plain program's by a relative error of at most 0.014.
Values may be sent and summed in bfloat16 or wider, within the bound.
A program may use at most 128 MiB of HBM per device.

v0:
```python
import jax
import jax.numpy as jnp
from jax import lax
from jax.sharding import PartitionSpec as P

CW = 512


clamp_limit = 7.0
glu_alpha = 1.702
norm_eps = 1e-05


def sent_together(arrays, axis, split_dim, concat_dim, along):
    ends, at = ([], 0)
    for a in arrays[:-1]:
        at += a.shape[along]
        ends.append(at)
    both = jnp.concatenate(arrays, axis=along)
    return tuple(
        jnp.split(
            lax.all_to_all(both, axis, split_axis=split_dim, concat_axis=concat_dim, tiled=True),
            ends,
            axis=along,
        )
    )


def sent_together_2(arrays, axis, dim, along):
    both = jnp.concatenate(arrays, axis=along)
    filled, at, finished = (lax.all_gather(both, axis, axis=dim, tiled=True), 0, [])
    for a in arrays:
        finished.append(lax.slice_in_dim(filled, at, at + a.shape[along], axis=along))
        at += a.shape[along]
    return tuple(finished)


def copy_for_each(shard, axis):
    size = lax.axis_size(axis)
    return lax.all_to_all(
        jnp.broadcast_to(shard[None], (size, *shard.shape)), axis, 0, 0, tiled=True
    )


def laid_out(tiles, dim):
    tiles = jnp.moveaxis(tiles, 0, dim)
    shape = tiles.shape
    return tiles.reshape(*shape[:dim], shape[dim] * shape[dim + 1], *shape[dim + 2 :])


def gather_directly(shard, axis, dim):
    tiles = copy_for_each(shard, axis)
    return laid_out(tiles, dim)


def taken_together(shard, axis):
    return copy_for_each(shard, axis).sum(axis=0)


def packed_total(arrays, axis):
    ends = [0]
    for a in arrays:
        ends.append(ends[-1] + a.size)
    so_far = taken_together(jnp.concatenate([a.ravel() for a in arrays]), axis)
    return tuple((so_far[b:e].reshape(a.shape) for a, b, e in zip(arrays, ends, ends[1:])))


def passed_along(shard, axis, by):
    size = lax.axis_size(axis)
    pairs = [(i, i + by) for i in range(size) if 0 <= i + by < size]
    return lax.ppermute(shard, axis, pairs)


def in_blocks(shard, dim, size):
    before, after = (shard.shape[:dim], shard.shape[dim + 1 :])
    return jnp.moveaxis(shard.reshape(*before, size, -1, *after), dim, 0)


def sum_at_owner(shard, axis, dim):
    tiles = in_blocks(shard, dim, lax.axis_size(axis))
    arrived = lax.all_to_all(tiles, axis, split_axis=0, concat_axis=0, tiled=True)
    return arrived.sum(axis=0)


def contract_rows(left, right):
    return lax.dot_general(
        left, right, (((0,), (0,)), ((), ())), preferred_element_type=jnp.float32
    )


def times_transposed(left, right):
    return lax.dot_general(
        left, right, (((1,), (1,)), ((), ())), preferred_element_type=jnp.float32
    )


def block_slots(block_routes, expert_count, capacity):
    flat_routes = block_routes.reshape(-1)
    one_hot = (flat_routes[:, None] == jnp.arange(expert_count, dtype=jnp.int32)[None, :]).astype(
        jnp.int32
    )
    earlier = jnp.cumsum(one_hot, axis=0) - one_hot
    slot_index = jnp.sum(earlier * one_hot, axis=1)
    target = flat_routes * capacity + slot_index
    pair_count = flat_routes.shape[0]
    table = (
        jnp.full((expert_count * capacity,), pair_count, jnp.int32)
        .at[target]
        .set(jnp.arange(pair_count, dtype=jnp.int32))
    )
    return (target, table)


def gather_pairs(table, block_stream, block_upstream, block_weights, topk):
    token_of = table // topk
    zero_row = jnp.zeros((1, block_stream.shape[1]), jnp.bfloat16)
    stream_pad = jnp.concatenate([block_stream, zero_row], axis=0)
    upstream_pad = jnp.concatenate([block_upstream, zero_row], axis=0)
    weight_pad = jnp.concatenate([block_weights.reshape(-1), jnp.zeros((1,), jnp.float32)])
    send_rows = stream_pad[token_of]
    send_cot = (weight_pad[table][:, None] * upstream_pad[token_of].astype(jnp.float32)).astype(
        jnp.bfloat16
    )
    return (send_rows, send_cot)


def expert_backward(expert_rows, expert_cot, gate_weight, up_weight, down_weight):
    gate_pre = jnp.dot(expert_rows, gate_weight, preferred_element_type=jnp.float32)
    up_pre = jnp.dot(expert_rows, up_weight, preferred_element_type=jnp.float32)
    capped = jnp.minimum(gate_pre, clamp_limit)
    clipped = jnp.clip(up_pre, -clamp_limit, clamp_limit)
    gate_sigmoid = jax.nn.sigmoid(glu_alpha * capped)
    act = (capped * gate_sigmoid * (clipped + 1.0)).astype(jnp.bfloat16)
    grad_down = contract_rows(act, expert_cot)
    grad_act = times_transposed(expert_cot, down_weight)
    slope = gate_sigmoid + glu_alpha * capped * gate_sigmoid * (1.0 - gate_sigmoid)
    grad_gate_pre = jnp.where(
        gate_pre < clamp_limit, grad_act * (clipped + 1.0) * slope, 0.0
    ).astype(jnp.bfloat16)
    grad_up_pre = jnp.where(
        jnp.abs(up_pre) < clamp_limit, grad_act * capped * gate_sigmoid, 0.0
    ).astype(jnp.bfloat16)
    grad_gate = contract_rows(expert_rows, grad_gate_pre)
    grad_up = contract_rows(expert_rows, grad_up_pre)
    return (grad_gate, grad_up, grad_down, grad_gate_pre, grad_up_pre)


def on_device(
    upstream,
    stream,
    routes,
    route_weights,
    glu_value,
    glu_gate,
    conv_taps,
    conv_saved,
    out_proj,
    expert_gate,
    expert_up,
    expert_down,
):
    tok_count = upstream.shape[0]
    model_width = upstream.shape[1]
    topk = routes.shape[1]
    expert_count = lax.axis_size("sp")
    capacity = 4 * tok_count // expert_count
    slice_width = model_width // lax.axis_size("tp")
    column_start = lax.axis_index("tp") * slice_width
    target, table = block_slots(routes, expert_count, capacity)
    stream_part = lax.dynamic_slice_in_dim(stream, column_start, slice_width, 1)
    upstream_part = lax.dynamic_slice_in_dim(upstream, column_start, slice_width, 1)
    send_rows, send_cot = gather_pairs(table, stream_part, upstream_part, route_weights, topk)
    part_shape = (expert_count, capacity, slice_width)
    part_rows, part_cot = sent_together(
        (send_rows.reshape(part_shape), send_cot.reshape(part_shape)), "sp", 0, 0, 1
    )
    got_rows, got_cot = sent_together_2((part_rows, part_cot), "tp", 2, 0)
    expert_rows = got_rows.reshape(-1, model_width)
    expert_cot = got_cot.reshape(-1, model_width)
    gate_weight = expert_gate[0]
    up_weight = expert_up[0]
    down_weight = expert_down[0]
    grad_gate_w, grad_up_w, grad_down_w, grad_gate_pre, grad_up_pre = expert_backward(
        expert_rows, expert_cot, gate_weight, up_weight, down_weight
    )
    partial_rows = times_transposed(grad_gate_pre, gate_weight) + times_transposed(
        grad_up_pre, up_weight
    )
    summed_rows = lax.psum_scatter(
        partial_rows.astype(jnp.bfloat16), "tp", scatter_dimension=1, tiled=True
    )
    returned = lax.all_to_all(
        summed_rows.reshape(expert_count, capacity, slice_width),
        "sp",
        split_axis=0,
        concat_axis=0,
        tiled=True,
    )
    pair_grads = returned.reshape(expert_count * capacity, slice_width)[target].astype(jnp.float32)
    routed_sum = jnp.sum(pair_grads.reshape(tok_count, topk, slice_width), axis=1)
    upstream_own = lax.dynamic_slice_in_dim(upstream, column_start, slice_width, 1)
    grad_stream = (upstream_own.astype(jnp.float32) + routed_sum).astype(jnp.bfloat16)
    full_grad = gather_directly(grad_stream, "tp", 1)
    saved_conv = conv_saved.astype(jnp.float32)
    total_sum, square_sum = packed_total(
        (jnp.sum(saved_conv, axis=1), jnp.sum(saved_conv * saved_conv, axis=1)), "tp"
    )
    mean_c = (total_sum / CW)[:, None]
    var_c = (square_sum / CW)[:, None] - mean_c * mean_c
    inv_std = lax.rsqrt(var_c + norm_eps)
    normed = (saved_conv - mean_c) * inv_std
    norm_sigmoid = jax.nn.sigmoid(normed)
    mixed = (normed * norm_sigmoid).astype(jnp.bfloat16)
    grad_mixed = jnp.dot(full_grad, out_proj, preferred_element_type=jnp.float32)
    grad_normed = grad_mixed * norm_sigmoid * (1.0 + normed * (1.0 - norm_sigmoid))
    first_sum, second_sum = packed_total(
        (jnp.sum(grad_normed, axis=1), jnp.sum(grad_normed * normed, axis=1)), "tp"
    )
    grad_conv = inv_std * (
        grad_normed - (first_sum / CW)[:, None] - normed * (second_sum / CW)[:, None]
    )
    kernel_width = conv_taps.shape[0]
    rim_rows = passed_along(grad_conv[: kernel_width - 1], "sp", -1)
    padded = jnp.concatenate([grad_conv, rim_rows], axis=0)
    grad_glu = jnp.zeros_like(grad_conv)
    for offset in range(kernel_width):
        grad_glu = grad_glu + conv_taps[offset][None, :] * padded[offset : offset + tok_count]
    gate_sig = jax.nn.sigmoid(glu_gate.astype(jnp.float32))
    grad_value = (grad_glu * gate_sig).astype(jnp.bfloat16)
    grad_gate = (grad_glu * glu_value.astype(jnp.float32) * gate_sig * (1.0 - gate_sig)).astype(
        jnp.bfloat16
    )
    grad_out_proj = sum_at_owner(contract_rows(full_grad, mixed), "sp", 0)
    return (
        grad_stream,
        grad_value,
        grad_gate,
        grad_out_proj,
        grad_gate_w[None],
        grad_up_w[None],
        grad_down_w[None],
    )


def solution(mesh):
    in_specs = (
        P("sp", None),
        P("sp", None),
        P("sp", None),
        P("sp", None),
        P("sp", "tp"),
        P("sp", "tp"),
        P(None, "tp"),
        P("sp", "tp"),
        P(None, "tp"),
        P("sp", None, "tp"),
        P("sp", None, "tp"),
        P("sp", "tp", None),
    )
    out_specs = (
        P("sp", "tp"),
        P("sp", "tp"),
        P("sp", "tp"),
        P("sp", "tp"),
        P("sp", None, "tp"),
        P("sp", None, "tp"),
        P("sp", "tp", None),
    )
    return jax.shard_map(
        on_device, mesh=mesh, in_specs=in_specs, out_specs=out_specs, check_vma=False
    )
```

profile of v0, /device:TPU:1, one launch (start us, length us, event | category | flops | bytes accessed | tf_op | source)
XLA Modules:
  0.0 267.9 jit_solution(10517415261337016135)
XLA Ops:
  9.4 1.2 reduce-window.6
  11.0 2.4 scatter_custom_fusion
  14.4 4.5 %gather_fusion.1 = f32[1024]{0:T(1024)S(1)} fusion(f32[513]{0:T(1024)S(1)} %pad_maximum_fusion.3, s32[1024]{0:T(1024)S(1)} %get-tuple-element.50), kind=kCustom, calls=%fused_computation.1 | custom fusion | bytes 12288 | tf_op jit(solution)/shard_map/gather | solution.py:121
  20.1 3.9 %gather_fusion.2 = bf16[1024,256]{1,0:T(8,128)(2,1)S(1)} fusion(bf16[257,256]{1,0:T(8,128)(2,1)S(1)} %concatenate.26, s32[1024]{0:T(1024)S(1)} %get-tuple-element.51), kind=kCustom, calls=%fused_computation.2 | custom fusion | bytes 1052672 | tf_op jit(solution)/shard_map/gather | solution.py:121
  24.0 3.9 %gather_fusion = bf16[1024,256]{1,0:T(8,128)(2,1)S(1)} fusion(bf16[257,256]{1,0:T(8,128)(2,1)S(1)} %concatenate.24, s32[1024]{0:T(1024)S(1)} %get-tuple-element.51), kind=kCustom, calls=%fused_computation | custom fusion | bytes 1052672 | tf_op jit(solution)/shard_map/gather | solution.py:120
  28.3 37.9 %all_to_all.32 = bf16[32,64,256]{2,1,0:T(8,128)(2,1)S(1)} all-to-all(bf16[32,64,256]{2,1,0:T(8,128)(2,1)S(1)} %pad_maximum_fusion), channel_id=1, replica_groups=mesh['sp'=32,'tp'=8] {'sp'}, dimensions={0} | all-to-all | bytes 2097152 | tf_op jit(solution)/shard_map/all_to_all | solution.py:22
  66.2 1.1 pad_maximum_fusion.1
  67.3 55.8 %all-gather.2.cloned.1.call-done = bf16[64,32,2048]{2,1,0:T(8,128)(2,1)} async-done(((bf16[64,32,256]{2,1,0:T(8,128)(2,1)}), bf16[64,32,2048]{2,1,0:T(8,128)(2,1)}) %all-gather.2.cloned.1.call-update) | async-done | bytes 8388624 | tf_op jit(solution)/shard_map/all_gather | solution.py:31
  123.2 4.0 %fusion.142 = (bf16[32,32,2048]{2,1,0:T(8,128)(2,1)S(1)}, bf16[32,32,2048]{2,1,0:T(8,128)(2,1)S(1)}) fusion(bf16[64,32,2048]{2,1,0:T(8,128)(2,1)} %all-gather.2.cloned.1.call-done), kind=kLoop, calls=%fused_computation.280 | loop fusion | bytes 16777216 | tf_op jit(solution)/shard_map/slice | solution.py:33
  127.2 1.3 fusion.3
  128.5 1.3 fusion.9
  130.5 1.9 select_convert_fusion
  132.4 1.3 fusion.7
  133.7 3.4 %add_convert_fusion = bf16[1024,2048]{1,0:T(8,128)(2,1)} fusion(f32[1024,2048]{1,0:T(8,128)S(1)} %fusion.7, bf16[1024,256]{1,0:T(8,128)(2,1)S(1)} %get-tuple-element.15, bf16[1,2048,256]{2,1,0:T(8,128)(2,1)S(1)} %copy-done.4), kind=kOutput, calls=%fused_computation.5 | convolution fusion | flops 1077936128 | bytes 14155776 | tf_op jit(solution)/shard_map/dot_general | solution.py:92
  137.9 8.7 %all_to_all.33 = f32[8,1,512]{2,1,0:T(1,128)S(1)} all-to-all(f32[8,1,512]{2,1,0:T(1,128)S(1)} %broadcast_in_dim.27), channel_id=1, replica_groups=mesh['sp'=32,'tp'=8] {'tp'}, dimensions={0} | all-to-all | bytes 32768 | tf_op jit(solution)/shard_map/all_to_all | solution.py:40
  146.6 29.0 %reduce-scatter.2.cloned.1.call-done = bf16[1024,256]{1,0:T(8,128)(2,1)} async-done(((bf16[1024,2048]{1,0:T(8,128)(2,1)}), bf16[1024,256]{1,0:T(8,128)(2,1)}) %reduce-scatter.2.cloned.1.call-update) | async-done | bytes 524304 | tf_op jit(solution)/shard_map/reduce_scatter | solution.py:189
  175.6 9.6 %all-to-all-start.1 = ((bf16[32,32,256]{2,1,0:T(8,128)(2,1)}), bf16[32,32,256]{2,1,0:T(8,128)(2,1)S(1)}, u32[]{:S(2)}, u32[]{:S(2)}) async-start(bf16[32,32,256]{2,1,0:T(8,128)(2,1)} %bitcast.146), calls=%async_computation.2 | async-start | bytes 1048576 | tf_op jit(solution)/shard_map/all_to_all | solution.py:192
  185.3 12.7 %all-to-all-done.1 = bf16[32,32,256]{2,1,0:T(8,128)(2,1)S(1)} async-done(((bf16[32,32,256]{2,1,0:T(8,128)(2,1)}), bf16[32,32,256]{2,1,0:T(8,128)(2,1)S(1)}, u32[]{:S(2)}, u32[]{:S(2)}) %all-to-all-start.1) | async-done | bytes 524320 | tf_op jit(solution)/shard_map/all_to_all | solution.py:192
  198.0 1.9 gather_fusion.3
  202.1 9.7 %all-to-all-start.3 = ((bf16[8,256,256]{1,2,0:T(8,128)(2,1)}), bf16[8,256,256]{1,2,0:T(8,128)(2,1)S(1)}, u32[]{:S(2)}, u32[]{:S(2)}) async-start(bf16[8,256,256]{1,2,0:T(8,128)(2,1)} %broadcast_in_dim.28), calls=%async_computation.4 | async-start | bytes 2097152 | tf_op jit(solution)/shard_map/all_to_all | solution.py:40
  211.8 5.0 %convolution_bitcast_fusion.1 = f32[1,2048,256]{2,1,0:T(8,128)} fusion(bf16[1024,2048]{1,0:T(8,128)(2,1)} %bitcast.140, bf16[1024,256]{1,0:T(8,128)(2,1)S(1)} %get-tuple-element.15), kind=kOutput, calls=%fused_computation.7 | convolution fusion | flops 1073741824 | bytes 6815744 | tf_op jit(solution)/shard_map/dot_general | solution.py:86
  216.8 2.8 %convolution_bitcast_fusion = f32[1,256,2048]{2,1,0:T(8,128)} fusion(bf16[1024,2048]{1,0:T(8,128)(2,1)S(1)} %bitcast.143, f32[1024,256]{1,0:T(8,128)S(1)} %copy-done.16, f32[1024,256]{1,0:T(8,128)S(1)} %copy-done.14), kind=kOutput, calls=%fused_computation.6 | convolution fusion | flops 1076363264 | bytes 8388608 | tf_op jit(solution)/shard_map/dot_general | solution.py:86
  219.7 7.1 %all-to-all-done.3 = bf16[8,256,256]{1,2,0:T(8,128)(2,1)S(1)} async-done(((bf16[8,256,256]{1,2,0:T(8,128)(2,1)}), bf16[8,256,256]{1,2,0:T(8,128)(2,1)S(1)}, u32[]{:S(2)}, u32[]{:S(2)}) %all-to-all-start.3) | async-done | bytes 1048608 | tf_op jit(solution)/shard_map/all_to_all | solution.py:40
  227.7 4.2 %all-to-all-start.4 = ((f32[8,1,512]{2,1,0:T(1,128)}), f32[8,1,512]{2,1,0:T(1,128)S(1)}, u32[]{:S(2)}, u32[]{:S(2)}) async-start(f32[8,1,512]{2,1,0:T(1,128)} %broadcast_in_dim.29), calls=%async_computation.5 | async-start | bytes 32768 | tf_op jit(solution)/shard_map/all_to_all | solution.py:40
  232.4 1.5 reshape.175
  233.8 2.8 %all-to-all-done.4 = f32[8,1,512]{2,1,0:T(1,128)S(1)} async-done(((f32[8,1,512]{2,1,0:T(1,128)}), f32[8,1,512]{2,1,0:T(1,128)S(1)}, u32[]{:S(2)}, u32[]{:S(2)}) %all-to-all-start.4) | async-done | bytes 16416 | tf_op jit(solution)/shard_map/all_to_all | solution.py:40
  236.6 4.6 %all-to-all-start.5 = ((f32[32,1,4096]{2,1,0:T(1,128)}), f32[32,1,4096]{2,1,0:T(1,128)S(1)}, u32[]{:S(2)}, u32[]{:S(2)}) async-start(f32[32,1,4096]{2,1,0:T(1,128)} %reshape.175), calls=%async_computation.6 | async-start | bytes 1048576 | tf_op jit(solution)/shard_map/all_to_all | solution.py:81
  241.3 1.3 collective-permute-start
  242.6 4.9 %convolution_bitcast_fusion.2 = f32[1,2048,256]{2,1,0:T(8,128)} fusion(bf16[1024,2048]{1,0:T(8,128)(2,1)} %bitcast.141, bf16[1024,256]{1,0:T(8,128)(2,1)} %copy-done.5), kind=kOutput, calls=%fused_computation.8 | convolution fusion | flops 1073741824 | bytes 6815744 | tf_op jit(solution)/shard_map/dot_general | solution.py:86
  247.6 1.8 multiply_convert_fusion.2
  250.0 7.5 %all-to-all-done.5 = f32[32,1,4096]{2,1,0:T(1,128)S(1)} async-done(((f32[32,1,4096]{2,1,0:T(1,128)}), f32[32,1,4096]{2,1,0:T(1,128)S(1)}, u32[]{:S(2)}, u32[]{:S(2)}) %all-to-all-start.5) | async-done | bytes 524320 | tf_op jit(solution)/shard_map/all_to_all | solution.py:81
  258.0 1.9 reduce.4
  (88 shorter events, 12.4 us)
Async XLA Ops:
  7.2 121.3 %copy-start = (bf16[1,2048,256]{2,1,0:T(8,128)(2,1)S(1)}, bf16[1,2048,256]{2,1,0:T(8,128)(2,1)}, u32[]{:S(2)}) copy-start(bf16[1,2048,256]{2,1,0:T(8,128)(2,1)} %param.21) | copy-start | bytes 3145732
  7.2 116.0 %all-gather.2.cloned.1.call-start = ((), (), s32[]{:S(2)}) async-start(), calls=%async_computation.7 | async-start | bytes 9437184 | tf_op jit(solution)/shard_map/all_gather | solution.py:31
  67.3 59.9 %copy-start.4 = (bf16[1,2048,256]{2,1,0:T(8,128)(2,1)S(1)}, bf16[1,2048,256]{2,1,0:T(8,128)(2,1)}, u32[]{:S(2)}) copy-start(bf16[1,2048,256]{2,1,0:T(8,128)(2,1)} %param.22) | copy-start | bytes 3145732
  67.3 108.3 %reduce-scatter.2.cloned.1.call-start = ((), (), s32[]{:S(2)}) async-start(), calls=%async_computation.8 | async-start | bytes 4718592 | tf_op jit(solution)/shard_map/reduce_scatter | solution.py:189
  127.2 2.6 copy-start.1
  127.2 3.2 %copy-start.2 = (bf16[32,32,2048]{2,1,0:T(8,128)(2,1)}, bf16[32,32,2048]{2,1,0:T(8,128)(2,1)S(1)}, u32[]{:S(2)}) copy-start(bf16[32,32,2048]{2,1,0:T(8,128)(2,1)S(1)} %get-tuple-element.14) | copy-start | bytes 12582916
  128.5 3.9 %copy-start.13 = (f32[1024,256]{1,0:T(8,128)}, f32[1024,256]{1,0:T(8,128)S(1)}, u32[]{:S(2)}) copy-start(f32[1024,256]{1,0:T(8,128)S(1)} %fusion.3) | copy-start | bytes 3145732
  128.5 2.0 copy-start.12
  129.8 2.6 copy-start.15
  132.4 1.3 copy-start.5
  137.1 0.8 copy-start.6
  137.1 48.1 %copy-start.11 = (f32[31,64]{1,0:T(8,128)S(1)}, f32[31,64]{1,0:T(8,128)}, u32[]{:S(2)}) copy-start(f32[31,64]{1,0:T(8,128)} %param.18) | copy-start | bytes 23812
  175.6 22.4 %all-to-all-start.1 = ((bf16[32,32,256]{2,1,0:T(8,128)(2,1)}), bf16[32,32,256]{2,1,0:T(8,128)(2,1)S(1)}, u32[]{:S(2)}, u32[]{:S(2)}) async-start(bf16[32,32,256]{2,1,0:T(8,128)(2,1)} %bitcast.146), calls=%async_computation.2 | async-start | bytes 1048576 | tf_op jit(solution)/shard_map/all_to_all | solution.py:192
  200.9 15.9 %copy-start.7 = (bf16[256,256]{1,0:T(8,128)(2,1)}, bf16[256,256]{1,0:T(8,128)(2,1)S(1)}, u32[]{:S(2)}) copy-start(bf16[256,256]{1,0:T(8,128)(2,1)S(1)} %add_convert_fusion.1) | copy-start | bytes 393220
  202.1 24.7 %all-to-all-start.3 = ((bf16[8,256,256]{1,2,0:T(8,128)(2,1)}), bf16[8,256,256]{1,2,0:T(8,128)(2,1)S(1)}, u32[]{:S(2)}, u32[]{:S(2)}) async-start(bf16[8,256,256]{1,2,0:T(8,128)(2,1)} %broadcast_in_dim.28), calls=%async_computation.4 | async-start | bytes 2097152 | tf_op jit(solution)/shard_map/all_to_all | solution.py:40
  211.8 5.0 %copy-start.3 = (bf16[32,32,2048]{2,1,0:T(8,128)(2,1)S(1)}, bf16[32,32,2048]{2,1,0:T(8,128)(2,1)}, u32[]{:S(2)}) copy-start(bf16[32,32,2048]{2,1,0:T(8,128)(2,1)} %copy-done.2) | copy-start | bytes 12582916
  211.8 5.0 %copy-start.14 = (f32[1024,256]{1,0:T(8,128)S(1)}, f32[1024,256]{1,0:T(8,128)}, u32[]{:S(2)}) copy-start(f32[1024,256]{1,0:T(8,128)} %copy-done.13) | copy-start | bytes 3145732
  211.8 5.0 %copy-start.16 = (f32[1024,256]{1,0:T(8,128)S(1)}, f32[1024,256]{1,0:T(8,128)}, u32[]{:S(2)}) copy-start(f32[1024,256]{1,0:T(8,128)} %copy-done.15) | copy-start | bytes 3145732
  216.8 10.0 %copy-start.8 = (bf16[2048,64]{0,1:T(8,128)(2,1)S(1)}, bf16[2048,64]{0,1:T(8,128)(2,1)}, u32[]{:S(2)}) copy-start(bf16[2048,64]{0,1:T(8,128)(2,1)} %param.20) | copy-start | bytes 786436
  227.7 8.9 %all-to-all-start.4 = ((f32[8,1,512]{2,1,0:T(1,128)}), f32[8,1,512]{2,1,0:T(1,128)S(1)}, u32[]{:S(2)}, u32[]{:S(2)}) async-start(f32[8,1,512]{2,1,0:T(1,128)} %broadcast_in_dim.29), calls=%async_computation.5 | async-start | bytes 32768 | tf_op jit(solution)/shard_map/all_to_all | solution.py:40
  236.6 20.9 %all-to-all-start.5 = ((f32[32,1,4096]{2,1,0:T(1,128)}), f32[32,1,4096]{2,1,0:T(1,128)S(1)}, u32[]{:S(2)}, u32[]{:S(2)}) async-start(f32[32,1,4096]{2,1,0:T(1,128)} %reshape.175), calls=%async_computation.6 | async-start | bytes 1048576 | tf_op jit(solution)/shard_map/all_to_all | solution.py:81
  241.3 6.3 %copy-start.9 = (bf16[256,64]{0,1:T(8,128)(2,1)S(1)}, bf16[256,64]{0,1:T(8,128)(2,1)}, u32[]{:S(2)}) copy-start(bf16[256,64]{0,1:T(8,128)(2,1)} %param.17) | copy-start | bytes 98308
  241.3 6.3 %copy-start.10 = (bf16[256,64]{0,1:T(8,128)(2,1)S(1)}, bf16[256,64]{0,1:T(8,128)(2,1)}, u32[]{:S(2)}) copy-start(bf16[256,64]{0,1:T(8,128)(2,1)} %param.16) | copy-start | bytes 98308
  241.3 6.2 %collective-permute-start = (f32[30,64]{0,1:T(8,128)S(1)}, f32[30,64]{0,1:T(8,128)S(1)}, u32[]{:S(2)}, u32[]{:S(2)}) collective-permute-start(f32[30,64]{0,1:T(8,128)S(1)} %slice.291), channel_id=1, source_target_pairs={{8,0},{16,8},{24,16},{32,24},{40,32},{48,40},{56,48},{64,56},{72,6... | collective-permute-start | bytes 23048 | tf_op jit(solution)/shard_map/ppermute | solution.py:71
Sparse Core Ops, SparseCore 0:
  67.4 55.7 all-gather.1
  137.3 38.3 reduce-scatter.1
where the time goes:
time: 269 us; the launch traced here: 268 us
  waiting for transfers between devices  115 us (43%)
  blocking collectives  46.6 us (17%)
  local copies, waits for them, and re-layouts  30.4 us (11%)
  starting transfers between devices  29.5 us (11%)
  matrix products  22.6 us (8%)
  between operations  14.6 us (5%)
  other arithmetic  9.25 us (3%)
    all_gather x1, waiting for transfers between devices, sent_together_2(): lax.all_gather(both, axis, axis=dim, tiled=True)  55.8 us
    all_to_all x1, blocking collectives, sent_together(): lax.all_to_all(both, axis, split_axis=split_dim, concat_axis=concat_dim,...  37.9 us
    reduce_scatter x1, waiting for transfers between devices, on_device(): lax.psum_scatter(partial_rows.astype(jnp.bfloat16), 'tp', scatter_dimensi...  29 us
    all_to_all x2, starting transfers between devices, copy_for_each(): lax.all_to_all(jnp.broadcast_to(shard[None], (size, *shard.shape)), axis,...  14 us
    dot_general x4, matrix products, contract_rows(): lax.dot_general(left, right, (((0,), (0,)), ((), ())), preferred_element_...  13.2 us
    all_to_all x1, waiting for transfers between devices, on_device(): lax.all_to_all(summed_rows.reshape(expert_count, capacity, slice_width),...  12.7 us
    all_to_all x2, waiting for transfers between devices, copy_for_each(): lax.all_to_all(jnp.broadcast_to(shard[None], (size, *shard.shape)), axis,...  9.9 us
    all_to_all x1, starting transfers between devices, on_device(): lax.all_to_all(summed_rows.reshape(expert_count, capacity, slice_width),...  9.58 us
  transfers between devices with their start and end apart: 7, of which 6 were waited for; matrix products, arithmetic and copies ran while one was open for 6% of the time, Pallas kernels for 0%

commit v1 on v0

v1 whole, which is shorter than its diff:
```python
import functools

import jax
import jax.numpy as jnp
from jax import lax
from jax.experimental import pallas as pl
from jax.experimental.pallas import tpu as pltpu
from jax.sharding import PartitionSpec as P

MESH = pl.DeviceIdType.MESH
BF16 = jnp.bfloat16
F32 = jnp.float32

CW = 512
NZ, NX, NY = 8, 4, 4
N_SP = 32
N_TP = 8
CAP = 32
TOK = 256
SL = 256
NC = 4
PER = N_SP // NC
ROWS = PER * CAP
HALF = ROWS // 2

clamp_limit = 7.0
glu_alpha = 1.702
norm_eps = 1e-05

DZ = (1, 7, 2, 6, 3, 5, 4, 0)
OWN = 28


def position_of(expert, z, x):
    dz = ((expert >> 2) - z) & 7
    dx = ((expert & 3) - x) & 3
    h = jnp.minimum(dz, 8 - dz)
    q = jnp.where(dz == 0, 7, jnp.where(dz == 4, 6, 2 * (h - 1) + jnp.where(dz > 4, 1, 0)))
    return 4 * q + dx


def dot_tn(left, right):
    return lax.dot_general(left, right, (((0,), (0,)), ((), ())), preferred_element_type=F32)


def dot_nt(left, right):
    return lax.dot_general(left, right, (((1,), (1,)), ((), ())), preferred_element_type=F32)


def dot_nn(left, right):
    return lax.dot_general(left, right, (((1,), (0,)), ((), ())), preferred_element_type=F32)


def main_kernel(
    up_hbm, st_hbm, routes_ref, weights_ref, wg_hbm, wu_hbm, wd_hbm,
    gs_ref, gg_hbm, gu_hbm, gd_hbm,
    up_v, st_v, wg, wu, wd, send, xs, onehot, part, part_in, comb, ring_in, relay, row_out, ret,
    acc_pre, ggp, gup, act_t, acc_g, acc_u, acc_d,
    load_sem, out_sem, a_snd, a_rcv, g_snd, g_rcv, r_snd, r_rcv, b_snd, b_rcv,
):
    sp = lax.axis_index("sp")
    tp = lax.axis_index("tp")
    z, x = sp // NX, sp % NX
    y, c = tp // 2, tp % 2
    fwd, bwd = ((y + 1) % NY) * 2 + c, ((y + 3) % NY) * 2 + c
    opp = ((y + 2) % NY) * 2 + c
    other = y * 2 + (1 - c)
    up_dev, down_dev, mate = (sp, fwd), (sp, bwd), (sp, other)
    oc = 1 - c
    fwd_o, bwd_o, opp_o = ((y + 1) % NY) * 2 + oc, ((y + 3) % NY) * 2 + oc, ((y + 2) % NY) * 2 + oc

    def sp_dev(p, sign):
        dz, dx = DZ[p // 4], p % 4
        if sign < 0:
            dz, dx = (NZ - dz) % NZ, (NX - dx) % NX
        return (((z + dz) % NZ) * NX + (x + dx) % NX, tp)

    column = pl.multiple_of(tp * SL, SL)
    loads = [
        pltpu.make_async_copy(st_hbm.at[:, pl.ds(column, SL)], st_v, load_sem.at[0]),
        pltpu.make_async_copy(up_hbm.at[:, pl.ds(column, SL)], up_v, load_sem.at[1]),
        pltpu.make_async_copy(wg_hbm, wg, load_sem.at[2]),
        pltpu.make_async_copy(wu_hbm, wu, load_sem.at[3]),
    ]
    for j in range(N_TP):
        loads.append(
            pltpu.make_async_copy(wd_hbm.at[:, pl.ds(j * SL, SL)], wd.at[j], load_sem.at[4 + j])
        )
    for copy in loads:
        copy.start()

    barrier = pltpu.get_barrier_semaphore()
    for p in range(N_SP):
        if p != OWN:
            pl.semaphore_signal(barrier, inc=1, device_id=sp_dev(p, 1), device_id_type=MESH)
    for dev in (up_dev, down_dev, mate):
        pl.semaphore_signal(barrier, inc=1, device_id=dev, device_id_type=MESH)

    r0, r1 = routes_ref[:, 0:1], routes_ref[:, 1:2]
    experts = lax.broadcasted_iota(jnp.int32, (TOK, N_SP), 1)
    c0 = jnp.where(r0 == experts, 1.0, 0.0).astype(F32)
    c1 = jnp.where(r1 == experts, 1.0, 0.0).astype(F32)
    tri = jnp.where(
        lax.broadcasted_iota(jnp.int32, (TOK, TOK), 1) < lax.broadcasted_iota(jnp.int32, (TOK, TOK), 0),
        1.0, 0.0,
    ).astype(BF16)
    earlier = dot_nn(tri, (c0 + c1).astype(BF16))
    slot0 = jnp.sum(earlier * c0, axis=1, keepdims=True).astype(jnp.int32)
    slot1 = jnp.sum(earlier * c1, axis=1, keepdims=True).astype(jnp.int32)
    pos0 = position_of(r0, z, x) * CAP + slot0
    pos1 = position_of(r1, z, x) * CAP + slot1
    loads[0].wait()
    loads[1].wait()
    stream = st_v[...]
    ups = up_v[...].astype(F32)
    cot0 = (weights_ref[:, 0:1] * ups).astype(BF16)
    cot1 = (weights_ref[:, 1:2] * ups).astype(BF16)
    lanes = lax.broadcasted_iota(jnp.int32, (TOK, ROWS), 1)

    def a2a(p):
        return pltpu.make_async_remote_copy(
            src_ref=send.at[p],
            dst_ref=xs.at[:, tp, pl.ds(p * CAP, CAP), :],
            send_sem=a_snd.at[p],
            recv_sem=a_rcv.at[p],
            device_id=sp_dev(p, 1),
            device_id_type=MESH,
        )

    for k in range(NC):
        s0 = jnp.where(pos0 - k * ROWS == lanes, 1.0, 0.0).astype(BF16)
        s1 = jnp.where(pos1 - k * ROWS == lanes, 1.0, 0.0).astype(BF16)
        both = s0 + s1
        onehot[k] = both
        rows = dot_tn(both, stream).astype(BF16)
        cots = (dot_tn(s0, cot0) + dot_tn(s1, cot1)).astype(BF16)
        send[k * PER:(k + 1) * PER, 0] = rows.reshape(PER, CAP, SL)
        send[k * PER:(k + 1) * PER, 1] = cots.reshape(PER, CAP, SL)
        if k == 0:
            pl.semaphore_wait(barrier, N_SP - 1 + 3)
        for p in range(k * PER, (k + 1) * PER):
            if p == OWN:
                xs[:, tp, pl.ds(p * CAP, CAP), :] = send[p]
            else:
                a2a(p).start()

    def gather(k, kind, rc, slice_at, dev):
        ref = xs.at[rc, slice_at, pl.ds(k * ROWS, ROWS), :]
        return pltpu.make_async_remote_copy(
            src_ref=ref, dst_ref=ref, send_sem=g_snd.at[k, kind], recv_sem=g_rcv.at[k, kind],
            device_id=dev, device_id_type=MESH,
        )

    plan = (
        (0, tp, up_dev), (0, tp, down_dev), (0, tp, mate),
        (1, tp, up_dev), (1, tp, down_dev), (1, tp, mate),
        (0, bwd, up_dev), (1, fwd, down_dev),
        (0, bwd, mate), (0, fwd, mate), (0, opp, mate),
        (1, fwd, mate), (1, bwd, mate), (1, opp, mate),
    )

    def spread(k, kind):
        rc, slice_at, dev = plan[kind]
        return gather(k, kind, rc, slice_at, dev)

    arrives = (bwd, fwd, other, bwd, fwd, other, opp, opp, bwd_o, fwd_o, opp_o, fwd_o, bwd_o, opp_o)
    arrives_rc = (0, 0, 0, 1, 1, 1, 0, 1, 0, 0, 0, 1, 1, 1)

    def got(k, kind):
        gather(k, kind, arrives_rc[kind], arrives[kind], mate).wait_recv()

    def stage_a(k):
        for p in range(k * PER, (k + 1) * PER):
            if p != OWN:
                a2a(p).wait_recv()
        for kind in (0, 4, 3, 1, 2, 5):
            spread(k, kind).start()

    def stage_b1(k):
        got(k, 0)
        spread(k, 6).start()
        got(k, 4)
        spread(k, 7).start()
        spread(k, 8).start()
        spread(k, 11).start()

    def stage_b2(k):
        got(k, 1)
        spread(k, 9).start()
        got(k, 3)
        spread(k, 12).start()
        got(k, 6)
        spread(k, 10).start()
        got(k, 7)
        spread(k, 13).start()

    def stage_b3(k):
        for kind in (2, 5, 8, 11, 9, 12, 10, 13):
            got(k, kind)

    def swap(k):
        return pltpu.make_async_remote_copy(
            src_ref=part.at[k, 1 - c], dst_ref=part_in.at[k],
            send_sem=r_snd.at[k, 0], recv_sem=r_rcv.at[k, 0], device_id=mate, device_id_type=MESH,
        )

    def stage_c(k):
        rows = pl.ds(k * ROWS, ROWS)
        acc_pre[...] = jnp.zeros_like(acc_pre)

        def pre(j, carry):
            r = xs[0, j, rows, :]
            acc_pre[0] += dot_nn(r, wg[j])
            acc_pre[1] += dot_nn(r, wu[j])
            acc_pre[2] += dot_nt(xs[1, j, rows, :], wd[j])
            return carry

        lax.fori_loop(0, N_TP, pre, 0)
        gate_pre, up_pre, grad_act = acc_pre[0], acc_pre[1], acc_pre[2]
        capped = jnp.minimum(gate_pre, clamp_limit)
        clipped = jnp.clip(up_pre, -clamp_limit, clamp_limit)
        sig = jax.nn.sigmoid(glu_alpha * capped)
        act = (capped * sig * (clipped + 1.0)).astype(BF16)
        slope = sig + glu_alpha * capped * sig * (1.0 - sig)
        g_gate = jnp.where(gate_pre < clamp_limit, grad_act * (clipped + 1.0) * slope, 0.0).astype(BF16)
        g_up = jnp.where(jnp.abs(up_pre) < clamp_limit, grad_act * capped * sig, 0.0).astype(BF16)
        act_t[k] = act
        ggp[k] = g_gate
        gup[k] = g_up

        def back(j, carry):
            total = dot_nt(ggp[k], wg[j]) + dot_nt(gup[k], wu[j])
            part[k, j % 2, j // 2] = total.astype(BF16)
            return carry

        lax.fori_loop(0, N_TP, back, 0)
        swap(k).start()

    def stage_w(k):
        rows = pl.ds(k * ROWS, ROWS)

        def grads(j, carry):
            r = xs[0, j, rows, :]
            g, u, d = dot_tn(r, ggp[k]), dot_tn(r, gup[k]), dot_tn(act_t[k], xs[1, j, rows, :])
            if k == 0:
                acc_g[j], acc_u[j], acc_d[j] = g, u, d
            else:
                acc_g[j] += g
                acc_u[j] += u
                acc_d[j] += d
            return carry

        lax.fori_loop(0, N_TP, grads, 0)

    lo, hi = pl.ds(0, HALF), pl.ds(HALF, HALF)

    def ring(k, kind, src, slot, dev):
        return pltpu.make_async_remote_copy(
            src_ref=src, dst_ref=ring_in.at[k, slot],
            send_sem=r_snd.at[k, kind], recv_sem=r_rcv.at[k, kind], device_id=dev, device_id_type=MESH,
        )

    def rings(k, kind):
        if kind == 0:
            return swap(k)
        if kind == 1:
            return ring(k, 1, comb.at[k, 2, lo, :], 0, down_dev)
        if kind == 2:
            return ring(k, 2, comb.at[k, 2, hi, :], 1, up_dev)
        if kind == 3:
            return ring(k, 3, comb.at[k, 1, lo, :], 2, up_dev)
        if kind == 4:
            return ring(k, 4, comb.at[k, 3, hi, :], 3, down_dev)
        if kind == 5:
            return ring(k, 5, relay.at[k, 0], 4, down_dev)
        return ring(k, 6, relay.at[k, 1], 5, up_dev)

    def stage_d(k):
        rings(k, 0).wait_recv()
        for r in (2, 1, 3, 0):
            at = (y + r) % NY
            comb[k, r] = (part[k, c, at].astype(F32) + part_in[k, at].astype(F32)).astype(BF16)
            if r == 2:
                rings(k, 1).start()
                rings(k, 2).start()
        rings(k, 3).start()
        rings(k, 4).start()

    def stage_e1(k):
        rings(k, 1).wait_recv()
        relay[k, 0] = (ring_in[k, 0].astype(F32) + comb[k, 3, lo, :].astype(F32)).astype(BF16)
        rings(k, 5).start()
        rings(k, 2).wait_recv()
        relay[k, 1] = (ring_in[k, 1].astype(F32) + comb[k, 1, hi, :].astype(F32)).astype(BF16)
        rings(k, 6).start()

    def back_copy(p):
        return pltpu.make_async_remote_copy(
            src_ref=row_out.at[p], dst_ref=ret.at[p],
            send_sem=b_snd.at[p], recv_sem=b_rcv.at[p], device_id=sp_dev(p, -1), device_id_type=MESH,
        )

    def stage_e2(k):
        for kind in (3, 4, 5, 6):
            rings(k, kind).wait_recv()
        low = comb[k, 0, lo, :].astype(F32) + ring_in[k, 2].astype(F32) + ring_in[k, 4].astype(F32)
        high = comb[k, 0, hi, :].astype(F32) + ring_in[k, 3].astype(F32) + ring_in[k, 5].astype(F32)
        at = k * PER
        row_out[at:at + PER // 2] = low.astype(BF16).reshape(PER // 2, CAP, SL)
        row_out[at + PER // 2:at + PER] = high.astype(BF16).reshape(PER // 2, CAP, SL)
        for p in range(at, at + PER):
            if p == OWN:
                ret[p] = row_out[p]
            else:
                back_copy(p).start()

    stage_a(0)
    stage_b1(0)
    stage_a(1)
    stage_b2(0)
    for copy in loads[2:]:
        copy.wait()
    stage_b3(0)
    stage_c(0)
    stage_b1(1)
    stage_a(2)
    stage_d(0)
    stage_b2(1)
    stage_b3(1)
    stage_c(1)
    stage_e1(0)
    stage_b1(2)
    stage_a(3)
    stage_d(1)
    stage_w(0)
    stage_e2(0)
    stage_b2(2)
    stage_b3(2)
    stage_c(2)
    stage_e1(1)
    stage_b1(3)
    stage_d(2)
    stage_w(1)
    stage_e2(1)
    stage_b2(3)
    stage_b3(3)
    stage_c(3)
    stage_e1(2)
    stage_d(3)
    stage_w(2)
    stage_e2(2)
    stage_e1(3)
    stage_w(3)
    outs = [
        pltpu.make_async_copy(acc_g, gg_hbm, out_sem.at[0]),
        pltpu.make_async_copy(acc_u, gu_hbm, out_sem.at[1]),
    ]
    for j in range(N_TP):
        outs.append(
            pltpu.make_async_copy(acc_d.at[j], gd_hbm.at[:, pl.ds(j * SL, SL)], out_sem.at[2 + j])
        )
    for copy in outs:
        copy.start()
    stage_e2(3)
    total = up_v[...].astype(F32)
    for k in range(NC):
        for p in range(k * PER, (k + 1) * PER):
            if p != OWN:
                back_copy(p).wait_recv()
        total = total + dot_nn(onehot[k], ret[k * PER:(k + 1) * PER].reshape(ROWS, SL))
    gs_ref[...] = total.astype(BF16)

    for p in range(N_SP):
        if p != OWN:
            a2a(p).wait_send()
            back_copy(p).wait_send()
    for k in range(NC):
        for kind in range(14):
            spread(k, kind).wait_send()
        for kind in range(7):
            rings(k, kind).wait_send()
    for copy in outs:
        copy.wait()


def main_call(upstream, stream, routes, route_weights, wg, wu, wd):
    any_spec = pl.BlockSpec(memory_space=pl.ANY)
    vmem = pl.BlockSpec(memory_space=pltpu.VMEM)
    flops = 2 * N_SP * CAP * 2048 * 256 * 8
    return pl.pallas_call(
        main_kernel,
        out_shape=(
            jax.ShapeDtypeStruct((TOK, SL), BF16),
            jax.ShapeDtypeStruct((N_TP, SL, SL), F32),
            jax.ShapeDtypeStruct((N_TP, SL, SL), F32),
            jax.ShapeDtypeStruct((SL, N_TP * SL), F32),
        ),
        in_specs=[any_spec, any_spec, vmem, vmem, any_spec, any_spec, any_spec],
        out_specs=(vmem, any_spec, any_spec, any_spec),
        scratch_shapes=[
            pltpu.VMEM((TOK, SL), BF16),
            pltpu.VMEM((TOK, SL), BF16),
            pltpu.VMEM((N_TP, SL, SL), BF16),
            pltpu.VMEM((N_TP, SL, SL), BF16),
            pltpu.VMEM((N_TP, SL, SL), BF16),
            pltpu.VMEM((N_SP, 2, CAP, SL), BF16),
            pltpu.VMEM((2, N_TP, N_SP * CAP, SL), BF16),
            pltpu.VMEM((NC, TOK, ROWS), BF16),
            pltpu.VMEM((NC, 2, NY, ROWS, SL), BF16),
            pltpu.VMEM((NC, NY, ROWS, SL), BF16),
            pltpu.VMEM((NC, NY, ROWS, SL), BF16),
            pltpu.VMEM((NC, 6, HALF, SL), BF16),
            pltpu.VMEM((NC, 2, HALF, SL), BF16),
            pltpu.VMEM((N_SP, CAP, SL), BF16),
            pltpu.VMEM((N_SP, CAP, SL), BF16),
            pltpu.VMEM((3, ROWS, SL), F32),
            pltpu.VMEM((NC, ROWS, SL), BF16),
            pltpu.VMEM((NC, ROWS, SL), BF16),
            pltpu.VMEM((NC, ROWS, SL), BF16),
            pltpu.VMEM((N_TP, SL, SL), F32),
            pltpu.VMEM((N_TP, SL, SL), F32),
            pltpu.VMEM((N_TP, SL, SL), F32),
            pltpu.SemaphoreType.DMA((12,)),
            pltpu.SemaphoreType.DMA((10,)),
            pltpu.SemaphoreType.DMA((N_SP,)),
            pltpu.SemaphoreType.DMA((N_SP,)),
            pltpu.SemaphoreType.DMA((NC, 14)),
            pltpu.SemaphoreType.DMA((NC, 14)),
            pltpu.SemaphoreType.DMA((NC, 7)),
            pltpu.SemaphoreType.DMA((NC, 7)),
            pltpu.SemaphoreType.DMA((N_SP,)),
            pltpu.SemaphoreType.DMA((N_SP,)),
        ],
        compiler_params=pltpu.CompilerParams(
            collective_id=0, has_side_effects=True, vmem_limit_bytes=56 * 1024 * 1024
        ),
        cost_estimate=pl.CostEstimate(flops=flops, bytes_accessed=16 << 20, transcendentals=0),
        name="routed_experts",
    )(upstream, stream, routes, route_weights, wg, wu, wd)


def copy_for_each(shard, axis):
    size = lax.axis_size(axis)
    return lax.all_to_all(
        jnp.broadcast_to(shard[None], (size, *shard.shape)), axis, 0, 0, tiled=True
    )


def laid_out(tiles, dim):
    tiles = jnp.moveaxis(tiles, 0, dim)
    shape = tiles.shape
    return tiles.reshape(*shape[:dim], shape[dim] * shape[dim + 1], *shape[dim + 2 :])


def gather_directly(shard, axis, dim):
    tiles = copy_for_each(shard, axis)
    return laid_out(tiles, dim)


def taken_together(shard, axis):
    return copy_for_each(shard, axis).sum(axis=0)


def packed_total(arrays, axis):
    ends = [0]
    for a in arrays:
        ends.append(ends[-1] + a.size)
    so_far = taken_together(jnp.concatenate([a.ravel() for a in arrays]), axis)
    return tuple((so_far[b:e].reshape(a.shape) for a, b, e in zip(arrays, ends, ends[1:])))


def passed_along(shard, axis, by):
    size = lax.axis_size(axis)
    pairs = [(i, i + by) for i in range(size) if 0 <= i + by < size]
    return lax.ppermute(shard, axis, pairs)


def in_blocks(shard, dim, size):
    before, after = (shard.shape[:dim], shard.shape[dim + 1 :])
    return jnp.moveaxis(shard.reshape(*before, size, -1, *after), dim, 0)


def sum_at_owner(shard, axis, dim):
    tiles = in_blocks(shard, dim, lax.axis_size(axis))
    arrived = lax.all_to_all(tiles, axis, split_axis=0, concat_axis=0, tiled=True)
    return arrived.sum(axis=0)


def contract_rows(left, right):
    return lax.dot_general(
        left, right, (((0,), (0,)), ((), ())), preferred_element_type=jnp.float32
    )


def on_device(
    upstream,
    stream,
    routes,
    route_weights,
    glu_value,
    glu_gate,
    conv_taps,
    conv_saved,
    out_proj,
    expert_gate,
    expert_up,
    expert_down,
):
    tok_count = upstream.shape[0]
    grad_stream, grad_gate_w, grad_up_w, grad_down_w = main_call(
        upstream, stream, routes, route_weights,
        expert_gate.reshape(N_TP, SL, SL), expert_up.reshape(N_TP, SL, SL), expert_down[0],
    )
    grad_gate_w = grad_gate_w.reshape(N_TP * SL, SL)
    grad_up_w = grad_up_w.reshape(N_TP * SL, SL)
    full_grad = gather_directly(grad_stream, "tp", 1)
    saved_conv = conv_saved.astype(jnp.float32)
    total_sum, square_sum = packed_total(
        (jnp.sum(saved_conv, axis=1), jnp.sum(saved_conv * saved_conv, axis=1)), "tp"
    )
    mean_c = (total_sum / CW)[:, None]
    var_c = (square_sum / CW)[:, None] - mean_c * mean_c
    inv_std = lax.rsqrt(var_c + norm_eps)
    normed = (saved_conv - mean_c) * inv_std
    norm_sigmoid = jax.nn.sigmoid(normed)
    mixed = (normed * norm_sigmoid).astype(jnp.bfloat16)
    grad_mixed = jnp.dot(full_grad, out_proj, preferred_element_type=jnp.float32)
    grad_normed = grad_mixed * norm_sigmoid * (1.0 + normed * (1.0 - norm_sigmoid))
    first_sum, second_sum = packed_total(
        (jnp.sum(grad_normed, axis=1), jnp.sum(grad_normed * normed, axis=1)), "tp"
    )
    grad_conv = inv_std * (
        grad_normed - (first_sum / CW)[:, None] - normed * (second_sum / CW)[:, None]
    )
    kernel_width = conv_taps.shape[0]
    rim_rows = passed_along(grad_conv[: kernel_width - 1], "sp", -1)
    padded = jnp.concatenate([grad_conv, rim_rows], axis=0)
    grad_glu = jnp.zeros_like(grad_conv)
    for offset in range(kernel_width):
        grad_glu = grad_glu + conv_taps[offset][None, :] * padded[offset : offset + tok_count]
    gate_sig = jax.nn.sigmoid(glu_gate.astype(jnp.float32))
    grad_value = (grad_glu * gate_sig).astype(jnp.bfloat16)
    grad_gate = (grad_glu * glu_value.astype(jnp.float32) * gate_sig * (1.0 - gate_sig)).astype(
        jnp.bfloat16
    )
    grad_out_proj = sum_at_owner(contract_rows(full_grad, mixed), "sp", 0)
    return (
        grad_stream,
        grad_value,
        grad_gate,
        grad_out_proj,
        grad_gate_w[None],
        grad_up_w[None],
        grad_down_w[None],
    )


def solution(mesh):
    in_specs = (
        P("sp", None),
        P("sp", None),
        P("sp", None),
        P("sp", None),
        P("sp", "tp"),
        P("sp", "tp"),
        P(None, "tp"),
        P("sp", "tp"),
        P(None, "tp"),
        P("sp", None, "tp"),
        P("sp", None, "tp"),
        P("sp", "tp", None),
    )
    out_specs = (
        P("sp", "tp"),
        P("sp", "tp"),
        P("sp", "tp"),
        P("sp", "tp"),
        P("sp", None, "tp"),
        P("sp", None, "tp"),
        P("sp", "tp", None),
    )
    return jax.shard_map(
        on_device, mesh=mesh, in_specs=in_specs, out_specs=out_specs, check_vma=False
    )
```

time: 269 us -> 169 us (0.63)
  Pallas kernels: 0 us -> 92.4 us
  waiting for transfers between devices: 115 us -> 30.1 us
  blocking collectives: 46.6 us -> 0 us
  matrix products: 22.6 us -> 0.72 us
  local copies, waits for them, and re-layouts: 30.4 us -> 16.2 us
  between operations: 14.6 us -> 0.8 us
  starting transfers between devices: 29.5 us -> 22.5 us
  other arithmetic: 9.25 us -> 5.9 us
    pallas_call x0 -> x1, Pallas kernels: none -> 92.4 us  [main_call(): pl.pallas_call(main_kernel, out_shape=(jax.ShapeDtypeStruct((TOK, SL), BF...]
    all_gather x1 -> x0, waiting for transfers between devices: 55.8 us -> none  [sent_together_2(): lax.all_gather(both, axis, axis=dim, tiled=True)]
    all_to_all x2 -> x0, blocking collectives: 46.6 us -> none  [the longest x1 37.9 us: sent_together(): lax.all_to_all(both, axis, split_axis=split_dim, concat_axis=concat_dim,...]
    reduce_scatter x1 -> x0, waiting for transfers between devices: 29 us -> none  [on_device(): lax.psum_scatter(partial_rows.astype(jnp.bfloat16), 'tp', scatter_dimensi...]
    gather x4 -> x0, local copies, waits for them, and re-layouts: 14.4 us -> none  [the longest x1 4.53 us: gather_pairs(): weight_pad[table][:, None] * upstream_pad[token_of].astype(jnp.float32)]
    dot_general x4 -> x1, matrix products: 13.2 us -> 0.42 us  [contract_rows(): lax.dot_general(left, right, (((0,), (0,)), ((), ())), preferred_element_...]
    all_to_all x1 -> x0, waiting for transfers between devices: 12.7 us -> none  [on_device(): lax.all_to_all(summed_rows.reshape(expert_count, capacity, slice_width),...]
    all_to_all x1 -> x0, starting transfers between devices: 9.58 us -> none  [on_device(): lax.all_to_all(summed_rows.reshape(expert_count, capacity, slice_width),...]
  transfers between devices with their start and end apart: 7 -> 5, of which waited for: 6 -> 4; matrix products, arithmetic and copies ran while one was open for 6% -> 5% of each run, Pallas kernels for 0% -> 55%
where the time goes in v1:
time: 169 us
  Pallas kernels  92.4 us (55%)
  waiting for transfers between devices  30.1 us (18%)
  starting transfers between devices  22.5 us (13%)
  local copies, waits for them, and re-layouts  16.2 us (10%)
  other arithmetic  5.9 us (3%)
    pallas_call x1, Pallas kernels, main_call(): pl.pallas_call(main_kernel, out_shape=(jax.ShapeDtypeStruct((TOK, SL), BF...  92.4 us
    all_to_all x3, waiting for transfers between devices, copy_for_each(): lax.all_to_all(jnp.broadcast_to(shard[None], (size, *shard.shape)), axis,...  17.7 us
    all_to_all x3, starting transfers between devices, copy_for_each(): lax.all_to_all(jnp.broadcast_to(shard[None], (size, *shard.shape)), axis,...  17.1 us
    unnamed x24, local copies, waits for them, and re-layouts  12.4 us
    all_to_all x1, waiting for transfers between devices, sum_at_owner(): lax.all_to_all(tiles, axis, split_axis=0, concat_axis=0, tiled=True)  8.68 us
    all_to_all x1, starting transfers between devices, sum_at_owner(): lax.all_to_all(tiles, axis, split_axis=0, concat_axis=0, tiled=True)  3.89 us
    ppermute x1, waiting for transfers between devices, passed_along(): return lax.ppermute(shard, axis, pairs)  3.67 us
  transfers between devices with their start and end apart: 5, of which 4 were waited for; matrix products, arithmetic and copies ran while one was open for 5% of the time, Pallas kernels for 55%

profile of v1, /device:TPU:1, one launch (start us, length us, event | category | flops | bytes accessed | tf_op | source)
XLA Modules:
  0.0 168.5 jit_solution(6478809344923676409)
XLA Ops:
  0.6 0.0 copy-start
  0.6 0.8 convert_reduce_fusion
  1.5 0.6 broadcast_in_dim.8
  2.1 6.4 %all-to-all-start = ((f32[8,1,512]{2,1,0:T(1,128)}), f32[8,1,512]{2,1,0:T(1,128)S(1)}, u32[]{:S(2)}, u32[]{:S(2)}) async-start(f32[8,1,512]{2,1,0:T(1,128)} %broadcast_in_dim.8), calls=%async_computation | async-start | bytes 32768 | tf_op jit(solution)/shard_map/all_to_all | solution.py:444
  8.5 1.5 copy.25.routes_ref
  10.0 1.5 copy.26.weights_ref
  11.5 92.4 %routed_experts.1 = (bf16[256,256]{1,0:T(8,128)(2,1)}, f32[8,256,256]{2,1,0:T(8,128)}, f32[8,256,256]{2,1,0:T(8,128)}, f32[256,2048]{1,0:T(8,128)}) custom-call(bf16[256,2048]{1,0:T(8,128)(2,1)} %up_hbm.1, bf16[256,2048]{1,0:T(8,128)(2,1)} %st_hbm.1, s32[256,2]{1,0:T(8,128)} %copy.25.routes_ref, f32[256,2]{1,0:T(8,128)} %copy.26.weights_ref, ...), custom_call_target="tpu_custom_call" | custom-call | flops 8589934592 | bytes 16777216 | tf_op jit(solution)/shard_map/routed_experts/pallas_call | solution.py:390
  103.9 1.0 copy.28
  104.9 1.0 broadcast_in_dim.9
  106.0 6.5 %all-to-all-start.1 = ((bf16[8,256,256]{1,2,0:T(8,128)(2,1)}), bf16[8,256,256]{1,2,0:T(8,128)(2,1)S(1)}, u32[]{:S(2)}, u32[]{:S(2)}) async-start(bf16[8,256,256]{1,2,0:T(8,128)(2,1)} %broadcast_in_dim.9), calls=%async_computation.1 | async-start | bytes 2097152 | tf_op jit(solution)/shard_map/all_to_all | solution.py:444
  112.5 14.9 %all-to-all-done.1 = bf16[8,256,256]{1,2,0:T(8,128)(2,1)S(1)} async-done(((bf16[8,256,256]{1,2,0:T(8,128)(2,1)}), bf16[8,256,256]{1,2,0:T(8,128)(2,1)S(1)}, u32[]{:S(2)}, u32[]{:S(2)}) %all-to-all-start.1) | async-done | bytes 1048608 | tf_op jit(solution)/shard_map/all_to_all | solution.py:444
  127.4 0.3 fusion.112
  127.7 0.6 broadcast_in_dim.10
  128.3 4.2 %all-to-all-start.2 = ((f32[8,1,512]{2,1,0:T(1,128)}), f32[8,1,512]{2,1,0:T(1,128)S(1)}, u32[]{:S(2)}, u32[]{:S(2)}) async-start(f32[8,1,512]{2,1,0:T(1,128)} %broadcast_in_dim.10), calls=%async_computation.2 | async-start | bytes 32768 | tf_op jit(solution)/shard_map/all_to_all | solution.py:444
  132.6 0.4 fusion.106
  133.0 1.5 reshape.50
  134.4 2.8 %all-to-all-done.2 = f32[8,1,512]{2,1,0:T(1,128)S(1)} async-done(((f32[8,1,512]{2,1,0:T(1,128)}), f32[8,1,512]{2,1,0:T(1,128)S(1)}, u32[]{:S(2)}, u32[]{:S(2)}) %all-to-all-start.2) | async-done | bytes 16416 | tf_op jit(solution)/shard_map/all_to_all | solution.py:444
  137.2 3.9 %all-to-all-start.3 = ((f32[32,1,4096]{2,1,0:T(1,128)}), f32[32,1,4096]{2,1,0:T(1,128)S(1)}, u32[]{:S(2)}, u32[]{:S(2)}) async-start(f32[32,1,4096]{2,1,0:T(1,128)} %reshape.50), calls=%async_computation.3 | async-start | bytes 1048576 | tf_op jit(solution)/shard_map/all_to_all | solution.py:485
  141.2 1.5 collective-permute-start
  142.7 3.7 %collective-permute-done = f32[30,64]{0,1:T(8,128)S(1)} collective-permute-done((f32[30,64]{0,1:T(8,128)S(1)}, f32[30,64]{0,1:T(8,128)S(1)}, u32[]{:S(2)}, u32[]{:S(2)}) %collective-permute-start) | collective-permute-done | bytes 7712 | tf_op jit(solution)/shard_map/ppermute | solution.py:475
  146.4 1.7 %multiply_convert_fusion = (bf16[256,64]{0,1:T(8,128)(2,1)}, f32[256,64]{0,1:T(8,128)S(1)}) fusion(bf16[256,64]{0,1:T(8,128)(2,1)S(1)} %copy-done.6, bf16[256,64]{0,1:T(8,128)(2,1)S(1)} %copy-done.5, f32[30,64]{0,1:T(8,128)S(1)} %collective-permute-done, f32[256,64]{0,1:T(8,128)S(1)} %fusion.14, f32[64]{0:T(128)S(1)} %get-tuple-element.50, ...), kind=kLoop, calls=%fused_computation.168 | loop fusion | flops 1654784 | bytes 244992 | tf_op jit(solution)/shard_map/convert_element_type | solution.py:543
  148.1 0.6 multiply_convert_fusion.1
  148.8 8.7 %all-to-all-done.3 = f32[32,1,4096]{2,1,0:T(1,128)S(1)} async-done(((f32[32,1,4096]{2,1,0:T(1,128)}), f32[32,1,4096]{2,1,0:T(1,128)S(1)}, u32[]{:S(2)}, u32[]{:S(2)}) %all-to-all-start.3) | async-done | bytes 524320 | tf_op jit(solution)/shard_map/all_to_all | solution.py:485
  157.4 0.5 broadcast.41
  158.0 1.9 %reduce.2 = f32[32,4096]{1,0:T(8,128)S(1)} reduce(f32[32,1,4096]{2,1,0:T(1,128)S(1)} %all-to-all-done.3, f32[]{:T(128)} %broadcast.41), dimensions={1}, to_apply=%all_to_all.17.reduce_sub_computation | reduce | bytes 1048580 | tf_op jit(solution)/shard_map/all_to_all | solution.py:485
  159.9 0.4 reshape.51
  160.3 0.7 reduce_sum.69
  161.0 0.7 copy.40
  161.6 3.2 %copy.41 = f32[1,2048,256]{2,1,0:T(8,128)} copy(f32[1,2048,256]{2,1,0:T(8,128)} %bitcast.85) | data formatting | bytes 4194304
  164.8 1.3 copy.42
  166.2 1.0 copy-done.1
  167.2 1.3 copy.43
  (25 shorter events, 0.2 us)
Async XLA Ops:
  0.6 126.8 %copy-start = (bf16[2048,64]{0,1:T(8,128)(2,1)S(1)}, bf16[2048,64]{0,1:T(8,128)(2,1)}, u32[]{:S(2)}) copy-start(bf16[2048,64]{0,1:T(8,128)(2,1)} %param.20) | copy-start | bytes 786436
  2.1 102.8 %all-to-all-start = ((f32[8,1,512]{2,1,0:T(1,128)}), f32[8,1,512]{2,1,0:T(1,128)S(1)}, u32[]{:S(2)}, u32[]{:S(2)}) async-start(f32[8,1,512]{2,1,0:T(1,128)} %broadcast_in_dim.8), calls=%async_computation | async-start | bytes 32768 | tf_op jit(solution)/shard_map/all_to_all | solution.py:444
  103.9 8.6 %copy-start.7 = (f32[31,64]{1,0:T(8,128)S(1)}, f32[31,64]{1,0:T(8,128)}, u32[]{:S(2)}) copy-start(f32[31,64]{1,0:T(8,128)} %param.18) | copy-start | bytes 23812
  103.9 23.5 %copy-start.3 = (bf16[256,64]{0,1:T(8,128)(2,1)S(1)}, bf16[256,64]{0,1:T(8,128)(2,1)}, u32[]{:S(2)}) copy-start(bf16[256,64]{0,1:T(8,128)(2,1)} %param.19) | copy-start | bytes 98308
  106.0 21.4 %all-to-all-start.1 = ((bf16[8,256,256]{1,2,0:T(8,128)(2,1)}), bf16[8,256,256]{1,2,0:T(8,128)(2,1)S(1)}, u32[]{:S(2)}, u32[]{:S(2)}) async-start(bf16[8,256,256]{1,2,0:T(8,128)(2,1)} %broadcast_in_dim.9), calls=%async_computation.1 | async-start | bytes 2097152 | tf_op jit(solution)/shard_map/all_to_all | solution.py:444
  128.3 8.9 %all-to-all-start.2 = ((f32[8,1,512]{2,1,0:T(1,128)}), f32[8,1,512]{2,1,0:T(1,128)S(1)}, u32[]{:S(2)}, u32[]{:S(2)}) async-start(f32[8,1,512]{2,1,0:T(1,128)} %broadcast_in_dim.10), calls=%async_computation.2 | async-start | bytes 32768 | tf_op jit(solution)/shard_map/all_to_all | solution.py:444
  132.6 13.8 %copy-start.5 = (bf16[256,64]{0,1:T(8,128)(2,1)S(1)}, bf16[256,64]{0,1:T(8,128)(2,1)}, u32[]{:S(2)}) copy-start(bf16[256,64]{0,1:T(8,128)(2,1)} %param.17) | copy-start | bytes 98308
  132.6 13.8 %copy-start.6 = (bf16[256,64]{0,1:T(8,128)(2,1)S(1)}, bf16[256,64]{0,1:T(8,128)(2,1)}, u32[]{:S(2)}) copy-start(bf16[256,64]{0,1:T(8,128)(2,1)} %param.16) | copy-start | bytes 98308
  137.2 20.2 %all-to-all-start.3 = ((f32[32,1,4096]{2,1,0:T(1,128)}), f32[32,1,4096]{2,1,0:T(1,128)S(1)}, u32[]{:S(2)}, u32[]{:S(2)}) async-start(f32[32,1,4096]{2,1,0:T(1,128)} %reshape.50), calls=%async_computation.3 | async-start | bytes 1048576 | tf_op jit(solution)/shard_map/all_to_all | solution.py:485
  141.2 5.2 %collective-permute-start = (f32[30,64]{0,1:T(8,128)S(1)}, f32[30,64]{0,1:T(8,128)S(1)}, u32[]{:S(2)}, u32[]{:S(2)}) collective-permute-start(f32[30,64]{0,1:T(8,128)S(1)} %slice.264), channel_id=1, source_target_pairs={{8,0},{16,8},{24,16},{32,24},{40,32},{48,40},{56,48},{64,56},{72,6... | collective-permute-start | bytes 23048 | tf_op jit(solution)/shard_map/ppermute | solution.py:475
  142.7 18.3 %copy-start.4 = (bf16[256,256]{1,0:T(8,128)(2,1)S(1)}, bf16[256,256]{1,0:T(8,128)(2,1)}, u32[]{:S(2)}) copy-start(bf16[256,256]{1,0:T(8,128)(2,1)} %get-tuple-element.64) | copy-start | bytes 393220
  161.6 3.2 %copy-start.2 = (f32[8,256,256]{2,1,0:T(8,128)S(1)}, f32[8,256,256]{2,1,0:T(8,128)}, u32[]{:S(2)}) copy-start(f32[8,256,256]{2,1,0:T(8,128)} %get-tuple-element.13) | copy-start | bytes 6291460
  164.8 2.3 %copy-start.1 = (f32[256,2048]{1,0:T(8,128)S(1)}, f32[256,2048]{1,0:T(8,128)}, u32[]{:S(2)}) copy-start(f32[256,2048]{1,0:T(8,128)} %get-tuple-element.14) | copy-start | bytes 6291460

commit v2 on v1

--- a/solution.py
+++ b/solution.py
@@ -1,5 +1,3 @@
-import functools
-
 import jax
 import jax.numpy as jnp
 from jax import lax
@@ -29,6 +27,8 @@
 
 DZ = (1, 7, 2, 6, 3, 5, 4, 0)
 OWN = 28
+CH = 64
+KW = 31
 
 
 def position_of(expert, z, x):
@@ -52,11 +52,15 @@
 
 
 def main_kernel(
-    up_hbm, st_hbm, routes_ref, weights_ref, wg_hbm, wu_hbm, wd_hbm,
-    gs_ref, gg_hbm, gu_hbm, gd_hbm,
-    up_v, st_v, wg, wu, wd, send, xs, onehot, part, part_in, comb, ring_in, relay, row_out, ret,
-    acc_pre, ggp, gup, act_t, acc_g, acc_u, acc_d,
-    load_sem, out_sem, a_snd, a_rcv, g_snd, g_rcv, r_snd, r_rcv, b_snd, b_rcv,
+    up_hbm, st_hbm, routes_hbm, weights_hbm, wg_hbm, wu_hbm, wd_hbm,
+    value_hbm, gate_hbm, taps_hbm, conv_hbm, proj_hbm,
+    gs_ref, gv_ref, gq_ref, go_ref, acc_g, acc_u, acc_d,
+    up_v, st_v, routes_v, weights_v, wg, wu, wd, send, xs, onehot, part, part_in, comb, ring_in, relay,
+    row_out, ret, acc_pre, ggp, gup, act_t,
+    value_v, gate_v, taps_v, conv_all, proj_all, hh, hn, mix, stat,
+    pm, pm_in, pm_out, pm_got, sums, sums_in, conv_grad, gt, gt_in, gt_out, gt_got,
+    load_sem, a_snd, a_rcv, g_snd, g_rcv, r_snd, r_rcv, b_snd, b_rcv,
+    e_snd, e_rcv, p_snd, p_rcv, s_snd, s_rcv, h_snd, h_rcv, o_snd, o_rcv, f_snd, f_rcv,
 ):
     sp = lax.axis_index("sp")
     tp = lax.axis_index("tp")
@@ -79,24 +83,47 @@
     loads = [
         pltpu.make_async_copy(st_hbm.at[:, pl.ds(column, SL)], st_v, load_sem.at[0]),
         pltpu.make_async_copy(up_hbm.at[:, pl.ds(column, SL)], up_v, load_sem.at[1]),
-        pltpu.make_async_copy(wg_hbm, wg, load_sem.at[2]),
-        pltpu.make_async_copy(wu_hbm, wu, load_sem.at[3]),
+        pltpu.make_async_copy(routes_hbm, routes_v, load_sem.at[2]),
+        pltpu.make_async_copy(weights_hbm, weights_v, load_sem.at[3]),
+    ]
+    late = [
+        pltpu.make_async_copy(wg_hbm, wg, load_sem.at[4]),
+        pltpu.make_async_copy(wu_hbm, wu, load_sem.at[5]),
     ]
     for j in range(N_TP):
-        loads.append(
-            pltpu.make_async_copy(wd_hbm.at[:, pl.ds(j * SL, SL)], wd.at[j], load_sem.at[4 + j])
-        )
-    for copy in loads:
+        late.append(
+            pltpu.make_async_copy(wd_hbm.at[:, pl.ds(j * SL, SL)], wd.at[j], load_sem.at[6 + j])
+        )
+    tail_loads = [
+        pltpu.make_async_copy(value_hbm, value_v, load_sem.at[14]),
+        pltpu.make_async_copy(gate_hbm, gate_v, load_sem.at[15]),
+        pltpu.make_async_copy(taps_hbm, taps_v, load_sem.at[16]),
+        pltpu.make_async_copy(conv_hbm, conv_all.at[tp], load_sem.at[17]),
+        pltpu.make_async_copy(proj_hbm.at[:, pl.ds(column, SL)], proj_all.at[tp], load_sem.at[18]),
+    ]
+    for copy in loads + late + tail_loads:
         copy.start()
 
     barrier = pltpu.get_barrier_semaphore()
     for p in range(N_SP):
         if p != OWN:
             pl.semaphore_signal(barrier, inc=1, device_id=sp_dev(p, 1), device_id_type=MESH)
-    for dev in (up_dev, down_dev, mate):
+    peers = [(sp, (tp + r) % N_TP) for r in range(1, N_TP)]
+    for dev in peers:
         pl.semaphore_signal(barrier, inc=1, device_id=dev, device_id_type=MESH)
-
-    r0, r1 = routes_ref[:, 0:1], routes_ref[:, 1:2]
+    owners = [(tp * NX + a, sp // NX) for a in range(NX)]
+    for a in range(NX):
+
+        @pl.when((sp // NX != tp) | (sp % NX != a))
+        def _(a=a):
+            pl.semaphore_signal(barrier, inc=1, device_id=owners[a], device_id_type=MESH)
+
+    for copy in loads:
+        copy.wait()
+    packed = jnp.concatenate(
+        [routes_v[...].astype(F32), weights_v[...], jnp.zeros((4, TOK), F32)], axis=0
+    ).T
+    r0, r1 = packed[:, 0:1].astype(jnp.int32), packed[:, 1:2].astype(jnp.int32)
     experts = lax.broadcasted_iota(jnp.int32, (TOK, N_SP), 1)
     c0 = jnp.where(r0 == experts, 1.0, 0.0).astype(F32)
     c1 = jnp.where(r1 == experts, 1.0, 0.0).astype(F32)
@@ -109,12 +136,10 @@
     slot1 = jnp.sum(earlier * c1, axis=1, keepdims=True).astype(jnp.int32)
     pos0 = position_of(r0, z, x) * CAP + slot0
     pos1 = position_of(r1, z, x) * CAP + slot1
-    loads[0].wait()
-    loads[1].wait()
     stream = st_v[...]
     ups = up_v[...].astype(F32)
-    cot0 = (weights_ref[:, 0:1] * ups).astype(BF16)
-    cot1 = (weights_ref[:, 1:2] * ups).astype(BF16)
+    cot0 = (packed[:, 2:3] * ups).astype(BF16)
+    cot1 = (packed[:, 3:4] * ups).astype(BF16)
     lanes = lax.broadcasted_iota(jnp.int32, (TOK, ROWS), 1)
 
     def a2a(p):
@@ -125,6 +150,15 @@
             recv_sem=a_rcv.at[p],
             device_id=sp_dev(p, 1),
             device_id_type=MESH,
+        )
+
+    def share(r, what):
+        at = pl.multiple_of(((tp + r) % N_TP) * SL, SL)
+        src = conv_hbm if what == 0 else proj_hbm.at[:, pl.ds(at, SL)]
+        dst = conv_all.at[tp] if what == 0 else proj_all.at[tp]
+        return pltpu.make_async_remote_copy(
+            src_ref=src, dst_ref=dst, send_sem=e_snd.at[what, r - 1], recv_sem=e_rcv.at[what, r - 1],
+            device_id=peers[r - 1], device_id_type=MESH,
         )
 
     for k in range(NC):
@@ -137,7 +171,17 @@
         send[k * PER:(k + 1) * PER, 0] = rows.reshape(PER, CAP, SL)
         send[k * PER:(k + 1) * PER, 1] = cots.reshape(PER, CAP, SL)
         if k == 0:
-            pl.semaphore_wait(barrier, N_SP - 1 + 3)
+            @pl.when(sp // NX == tp)
+            def _():
+                pl.semaphore_wait(barrier, N_SP + N_TP + NX - 3)
+
+            @pl.when(sp // NX != tp)
+            def _():
+                pl.semaphore_wait(barrier, N_SP + N_TP + NX - 2)
+
+            for r in range(1, N_TP):
+                share(r, 0).start()
+                share(r, 1).start()
         for p in range(k * PER, (k + 1) * PER):
             if p == OWN:
                 xs[:, tp, pl.ds(p * CAP, CAP), :] = send[p]
@@ -241,13 +285,14 @@
 
         def grads(j, carry):
             r = xs[0, j, rows, :]
+            at = pl.ds(pl.multiple_of(j * SL, SL), SL)
             g, u, d = dot_tn(r, ggp[k]), dot_tn(r, gup[k]), dot_tn(act_t[k], xs[1, j, rows, :])
             if k == 0:
-                acc_g[j], acc_u[j], acc_d[j] = g, u, d
+                acc_g[j], acc_u[j], acc_d[:, at] = g, u, d
             else:
                 acc_g[j] += g
                 acc_u[j] += u
-                acc_d[j] += d
+                acc_d[:, at] += d
             return carry
 
         lax.fori_loop(0, N_TP, grads, 0)
@@ -314,17 +359,41 @@
             else:
                 back_copy(p).start()
 
+    def stage_n():
+        for copy in tail_loads:
+            copy.wait()
+        for r in range(1, N_TP):
+            share(r, 0).wait_recv()
+            share(r, 1).wait_recv()
+        total, square = jnp.zeros((1, TOK), F32), jnp.zeros((1, TOK), F32)
+        for k in range(N_TP):
+            v = conv_all[k].astype(F32)
+            total = total + jnp.sum(v, axis=0, keepdims=True)
+            square = square + jnp.sum(v * v, axis=0, keepdims=True)
+        mean = total / CW
+        inv = lax.rsqrt(square / CW - mean * mean + norm_eps)
+        stat[0:1, :] = mean
+        stat[1:2, :] = inv
+        for k in range(N_TP):
+            n = (conv_all[k].astype(F32) - mean) * inv
+            sig = jax.nn.sigmoid(n)
+            slope = sig * (1.0 + n * (1.0 - sig))
+            mix[k] = (n * sig).astype(BF16)
+            hh[k] = slope
+            hn[k] = slope * n
+
     stage_a(0)
     stage_b1(0)
     stage_a(1)
     stage_b2(0)
-    for copy in loads[2:]:
+    for copy in late:
         copy.wait()
     stage_b3(0)
     stage_c(0)
     stage_b1(1)
     stage_a(2)
     stage_d(0)
+    stage_n()
     stage_b2(1)
     stage_b3(1)
     stage_c(1)
@@ -350,146 +419,236 @@
     stage_w(2)
     stage_e2(2)
     stage_e1(3)
+    stage_e2(3)
     stage_w(3)
-    outs = [
-        pltpu.make_async_copy(acc_g, gg_hbm, out_sem.at[0]),
-        pltpu.make_async_copy(acc_u, gu_hbm, out_sem.at[1]),
-    ]
-    for j in range(N_TP):
-        outs.append(
-            pltpu.make_async_copy(acc_d.at[j], gd_hbm.at[:, pl.ds(j * SL, SL)], out_sem.at[2 + j])
-        )
-    for copy in outs:
-        copy.start()
-    stage_e2(3)
     total = up_v[...].astype(F32)
     for k in range(NC):
         for p in range(k * PER, (k + 1) * PER):
             if p != OWN:
                 back_copy(p).wait_recv()
         total = total + dot_nn(onehot[k], ret[k * PER:(k + 1) * PER].reshape(ROWS, SL))
-    gs_ref[...] = total.astype(BF16)
+    grads = total.astype(BF16)
+    gs_ref[...] = grads
+
+    prod = dot_nt(proj_all[...].reshape(CW, SL), grads)
+    sums[0:1, :] = jnp.sum(prod * hh[...].reshape(CW, TOK), axis=0, keepdims=True)
+    sums[1:2, :] = jnp.sum(prod * hn[...].reshape(CW, TOK), axis=0, keepdims=True)
+    for k in range(N_TP):
+        pm[k % 2, k // 2] = prod[k * CH:(k + 1) * CH].astype(BF16)
+
+    def pm_copy(r):
+        if r == 0:
+            src, dst, dev = pm.at[1 - c], pm_in, mate
+        else:
+            src, dst, dev = pm_out.at[r - 1], pm_got.at[r - 1], (sp, ((y + r) % NY) * 2 + c)
+        return pltpu.make_async_remote_copy(
+            src_ref=src, dst_ref=dst, send_sem=p_snd.at[r], recv_sem=p_rcv.at[r],
+            device_id=dev, device_id_type=MESH,
+        )
+
+    def sum_copy(r):
+        return pltpu.make_async_remote_copy(
+            src_ref=sums, dst_ref=sums_in.at[r - 1], send_sem=s_snd.at[r - 1], recv_sem=s_rcv.at[r - 1],
+            device_id=peers[r - 1], device_id_type=MESH,
+        )
+
+    pm_copy(0).start()
+    for r in range(1, N_TP):
+        sum_copy(r).start()
+
+    gt[...] = dot_nn(mix[...].reshape(CW, TOK), grads).astype(BF16).reshape(N_SP, CW // N_SP, SL)
+
+    def gt_copy(p):
+        dev = sp_dev(p, 1)
+        return pltpu.make_async_remote_copy(
+            src_ref=gt.at[dev[0]], dst_ref=gt_in.at[p], send_sem=o_snd.at[p], recv_sem=o_rcv.at[p],
+            device_id=dev, device_id_type=MESH,
+        )
+
+    for p in range(N_SP):
+        if p != OWN:
+            gt_copy(p).start()
+
+    pm_copy(0).wait_recv()
+    for r in (2, 1, 3):
+        at = (y + r) % NY
+        pm_out[r - 1] = (pm[c, at].astype(F32) + pm_in[at].astype(F32)).astype(BF16)
+        pm_copy(r).start()
+    mixed_grad = pm[c, y].astype(F32) + pm_in[y].astype(F32)
+    first, second = sums[0:1, :], sums[1:2, :]
+    for r in range(1, N_TP):
+        sum_copy(r).wait_recv()
+        first = first + sums_in[r - 1, 0:1, :]
+        second = second + sums_in[r - 1, 1:2, :]
+    for r in (1, 3, 2):
+        pm_copy(r).wait_recv()
+        mixed_grad = mixed_grad + pm_got[r - 1].astype(F32)
+    mean, inv = stat[0:1, :], stat[1:2, :]
+    normed = (conv_all[tp].astype(F32) - mean) * inv
+    grad_normed = mixed_grad * hh[tp]
+    conv_grad[:, 0:TOK] = inv * (grad_normed - first / CW - normed * (second / CW))
+    halo = pltpu.make_async_remote_copy(
+        src_ref=conv_grad.at[:, pl.ds(0, 128)], dst_ref=conv_grad.at[:, pl.ds(TOK, 128)],
+        send_sem=h_snd, recv_sem=h_rcv, device_id=((sp + N_SP - 1) % N_SP, tp), device_id_type=MESH,
+    )
+    halo.start()
+
+    owned = gt[sp].astype(F32)
+    for p in range(N_SP):
+        if p != OWN:
+            gt_copy(p).wait_recv()
+            owned = owned + gt_in[p].astype(F32)
+    gt_out[0] = owned[:, 0:128]
+    gt_out[1] = owned[:, 128:256]
+    part_at = sp % NX
+
+    def owner_copy(a, slot):
+        return pltpu.make_async_remote_copy(
+            src_ref=gt_out.at[a // 2], dst_ref=gt_got.at[slot], send_sem=f_snd.at[a], recv_sem=f_rcv.at[slot],
+            device_id=owners[a], device_id_type=MESH,
+        )
+
+    for a in range(NX):
+        mine = (sp // NX == tp) & (part_at == a)
+
+        @pl.when(mine)
+        def _(a=a):
+            gt_got[a] = gt_out[a // 2]
+
+        @pl.when(jnp.logical_not(mine))
+        def _(a=a):
+            owner_copy(a, part_at).start()
+
+    halo.wait_recv()
+    tail = conv_grad[:, TOK:TOK + 128]
+    wide = jnp.concatenate([conv_grad[:, 0:TOK], jnp.where(sp == N_SP - 1, 0.0, tail)], axis=1)
+    taps_t = jnp.concatenate([taps_v[...], jnp.zeros((1, CH), F32)], axis=0).T
+    glu = taps_t[:, 0:1] * wide[:, 0:TOK]
+    for offset in range(1, KW):
+        glu = glu + taps_t[:, offset:offset + 1] * pltpu.roll(wide, TOK + 128 - offset, 1)[:, 0:TOK]
+    gate_sig = jax.nn.sigmoid(gate_v[...].astype(F32))
+    gv_ref[...] = (glu * gate_sig).astype(BF16)
+    gq_ref[...] = (glu * value_v[...].astype(F32) * gate_sig * (1.0 - gate_sig)).astype(BF16)
+
+    for a in range(NX):
+        mine = (sp // NX == tp) & (part_at == a)
+
+        @pl.when(jnp.logical_not(mine))
+        def _(a=a):
+            owner_copy(a, a).wait_recv()
+            owner_copy(a, part_at).wait_send()
+
+    got_t = gt_got[...].reshape(CH, 128).T
+    go_ref[...] = jnp.where(part_at % 2 == 0, got_t[0:CH, :], got_t[CH:2 * CH, :])
 
     for p in range(N_SP):
         if p != OWN:
             a2a(p).wait_send()
             back_copy(p).wait_send()
+            gt_copy(p).wait_send()
     for k in range(NC):
         for kind in range(14):
             spread(k, kind).wait_send()
         for kind in range(7):
             rings(k, kind).wait_send()
-    for copy in outs:
-        copy.wait()
-
-
-def main_call(upstream, stream, routes, route_weights, wg, wu, wd):
+    for r in range(NY):
+        pm_copy(r).wait_send()
+    for r in range(1, N_TP):
+        sum_copy(r).wait_send()
+        share(r, 0).wait_send()
+        share(r, 1).wait_send()
+    halo.wait_send()
+
+
+def main_call(*operands):
     any_spec = pl.BlockSpec(memory_space=pl.ANY)
     vmem = pl.BlockSpec(memory_space=pltpu.VMEM)
     flops = 2 * N_SP * CAP * 2048 * 256 * 8
+    V = pltpu.VMEM
+    D = pltpu.SemaphoreType.DMA
     return pl.pallas_call(
         main_kernel,
         out_shape=(
             jax.ShapeDtypeStruct((TOK, SL), BF16),
+            jax.ShapeDtypeStruct((CH, TOK), BF16),
+            jax.ShapeDtypeStruct((CH, TOK), BF16),
+            jax.ShapeDtypeStruct((CH, CH), F32),
             jax.ShapeDtypeStruct((N_TP, SL, SL), F32),
             jax.ShapeDtypeStruct((N_TP, SL, SL), F32),
             jax.ShapeDtypeStruct((SL, N_TP * SL), F32),
         ),
-        in_specs=[any_spec, any_spec, vmem, vmem, any_spec, any_spec, any_spec],
-        out_specs=(vmem, any_spec, any_spec, any_spec),
+        in_specs=[any_spec] * 12,
+        out_specs=(vmem,) * 7,
         scratch_shapes=[
-            pltpu.VMEM((TOK, SL), BF16),
-            pltpu.VMEM((TOK, SL), BF16),
-            pltpu.VMEM((N_TP, SL, SL), BF16),
-            pltpu.VMEM((N_TP, SL, SL), BF16),
-            pltpu.VMEM((N_TP, SL, SL), BF16),
-            pltpu.VMEM((N_SP, 2, CAP, SL), BF16),
-            pltpu.VMEM((2, N_TP, N_SP * CAP, SL), BF16),
-            pltpu.VMEM((NC, TOK, ROWS), BF16),
-            pltpu.VMEM((NC, 2, NY, ROWS, SL), BF16),
-            pltpu.VMEM((NC, NY, ROWS, SL), BF16),
-            pltpu.VMEM((NC, NY, ROWS, SL), BF16),
-            pltpu.VMEM((NC, 6, HALF, SL), BF16),
-            pltpu.VMEM((NC, 2, HALF, SL), BF16),
-            pltpu.VMEM((N_SP, CAP, SL), BF16),
-            pltpu.VMEM((N_SP, CAP, SL), BF16),
-            pltpu.VMEM((3, ROWS, SL), F32),
-            pltpu.VMEM((NC, ROWS, SL), BF16),
-            pltpu.VMEM((NC, ROWS, SL), BF16),
-            pltpu.VMEM((NC, ROWS, SL), BF16),
-            pltpu.VMEM((N_TP, SL, SL), F32),
-            pltpu.VMEM((N_TP, SL, SL), F32),
-            pltpu.VMEM((N_TP, SL, SL), F32),
-            pltpu.SemaphoreType.DMA((12,)),
-            pltpu.SemaphoreType.DMA((10,)),
-            pltpu.SemaphoreType.DMA((N_SP,)),
-            pltpu.SemaphoreType.DMA((N_SP,)),
-            pltpu.SemaphoreType.DMA((NC, 14)),
-            pltpu.SemaphoreType.DMA((NC, 14)),
-            pltpu.SemaphoreType.DMA((NC, 7)),
-            pltpu.SemaphoreType.DMA((NC, 7)),
-            pltpu.SemaphoreType.DMA((N_SP,)),
-            pltpu.SemaphoreType.DMA((N_SP,)),
+            V((TOK, SL), BF16),
+            V((TOK, SL), BF16),
+            V((2, TOK), jnp.int32),
+            V((2, TOK), F32),
+            V((N_TP, SL, SL), BF16),
+            V((N_TP, SL, SL), BF16),
+            V((N_TP, SL, SL), BF16),
+            V((N_SP, 2, CAP, SL), BF16),
+            V((2, N_TP, N_SP * CAP, SL), BF16),
+            V((NC, TOK, ROWS), BF16),
+            V((NC, 2, NY, ROWS, SL), BF16),
+            V((NC, NY, ROWS, SL), BF16),
+            V((NC, NY, ROWS, SL), BF16),
+            V((NC, 6, HALF, SL), BF16),
+            V((NC, 2, HALF, SL), BF16),
+            V((N_SP, CAP, SL), BF16),
+            V((N_SP, CAP, SL), BF16),
+            V((3, ROWS, SL), F32),
+            V((NC, ROWS, SL), BF16),
+            V((NC, ROWS, SL), BF16),
+            V((NC, ROWS, SL), BF16),
+            V((CH, TOK), BF16),
+            V((CH, TOK), BF16),
+            V((KW, CH), F32),
+            V((N_TP, CH, TOK), BF16),
+            V((N_TP, CH, SL), BF16),
+            V((N_TP, CH, TOK), F32),
+            V((N_TP, CH, TOK), F32),
+            V((N_TP, CH, TOK), BF16),
+            V((8, TOK), F32),
+            V((2, NY, CH, TOK), BF16),
+            V((NY, CH, TOK), BF16),
+            V((NY - 1, CH, TOK), BF16),
+            V((NY - 1, CH, TOK), BF16),
+            V((8, TOK), F32),
+            V((N_TP - 1, 8, TOK), F32),
+            V((CH, TOK + 128), F32),
+            V((N_SP, CW // N_SP, SL), BF16),
+            V((N_SP, CW // N_SP, SL), BF16),
+            V((2, CW // N_SP, 128), F32),
+            V((NX, CW // N_SP, 128), F32),
+            D((19,)),
+            D((N_SP,)),
+            D((N_SP,)),
+            D((NC, 14)),
+            D((NC, 14)),
+            D((NC, 7)),
+            D((NC, 7)),
+            D((N_SP,)),
+            D((N_SP,)),
+            D((2, N_TP - 1)),
+            D((2, N_TP - 1)),
+            D((NY,)),
+            D((NY,)),
+            D((N_TP - 1,)),
+            D((N_TP - 1,)),
+            D,
+            D,
+            D((N_SP,)),
+            D((N_SP,)),
+            D((NX,)),
+            D((NX,)),
         ],
         compiler_params=pltpu.CompilerParams(
-            collective_id=0, has_side_effects=True, vmem_limit_bytes=56 * 1024 * 1024
+            collective_id=0, has_side_effects=True, vmem_limit_bytes=60 * 1024 * 1024
         ),
         cost_estimate=pl.CostEstimate(flops=flops, bytes_accessed=16 << 20, transcendentals=0),
         name="routed_experts",
-    )(upstream, stream, routes, route_weights, wg, wu, wd)
-
-
-def copy_for_each(shard, axis):
-    size = lax.axis_size(axis)
-    return lax.all_to_all(
-        jnp.broadcast_to(shard[None], (size, *shard.shape)), axis, 0, 0, tiled=True
-    )
-
-
-def laid_out(tiles, dim):
-    tiles = jnp.moveaxis(tiles, 0, dim)
-    shape = tiles.shape
-    return tiles.reshape(*shape[:dim], shape[dim] * shape[dim + 1], *shape[dim + 2 :])
-
-
-def gather_directly(shard, axis, dim):
-    tiles = copy_for_each(shard, axis)
-    return laid_out(tiles, dim)
-
-
-def taken_together(shard, axis):
-    return copy_for_each(shard, axis).sum(axis=0)
-
-
-def packed_total(arrays, axis):
-    ends = [0]
-    for a in arrays:
-        ends.append(ends[-1] + a.size)
-    so_far = taken_together(jnp.concatenate([a.ravel() for a in arrays]), axis)
-    return tuple((so_far[b:e].reshape(a.shape) for a, b, e in zip(arrays, ends, ends[1:])))
-
-
-def passed_along(shard, axis, by):
-    size = lax.axis_size(axis)
-    pairs = [(i, i + by) for i in range(size) if 0 <= i + by < size]
-    return lax.ppermute(shard, axis, pairs)
-
-
-def in_blocks(shard, dim, size):
-    before, after = (shard.shape[:dim], shard.shape[dim + 1 :])
-    return jnp.moveaxis(shard.reshape(*before, size, -1, *after), dim, 0)
-
-
-def sum_at_owner(shard, axis, dim):
-    tiles = in_blocks(shard, dim, lax.axis_size(axis))
-    arrived = lax.all_to_all(tiles, axis, split_axis=0, concat_axis=0, tiled=True)
-    return arrived.sum(axis=0)
-
-
-def contract_rows(left, right):
-    return lax.dot_general(
-        left, right, (((0,), (0,)), ((), ())), preferred_element_type=jnp.float32
-    )
+    )(*operands)
 
 
 def on_device(
@@ -506,51 +665,18 @@
     expert_up,
     expert_down,
 ):
-    tok_count = upstream.shape[0]
-    grad_stream, grad_gate_w, grad_up_w, grad_down_w = main_call(
-        upstream, stream, routes, route_weights,
+    grad_stream, grad_value, grad_gate, grad_out_proj, grad_gate_w, grad_up_w, grad_down_w = main_call(
+        upstream, stream, routes.T, route_weights.T,
         expert_gate.reshape(N_TP, SL, SL), expert_up.reshape(N_TP, SL, SL), expert_down[0],
+        glu_value.T, glu_gate.T, conv_taps, conv_saved.T, out_proj.T,
     )
-    grad_gate_w = grad_gate_w.reshape(N_TP * SL, SL)
-    grad_up_w = grad_up_w.reshape(N_TP * SL, SL)
-    full_grad = gather_directly(grad_stream, "tp", 1)
-    saved_conv = conv_saved.astype(jnp.float32)
-    total_sum, square_sum = packed_total(
-        (jnp.sum(saved_conv, axis=1), jnp.sum(saved_conv * saved_conv, axis=1)), "tp"
-    )
-    mean_c = (total_sum / CW)[:, None]
-    var_c = (square_sum / CW)[:, None] - mean_c * mean_c
-    inv_std = lax.rsqrt(var_c + norm_eps)
-    normed = (saved_conv - mean_c) * inv_std
-    norm_sigmoid = jax.nn.sigmoid(normed)
-    mixed = (normed * norm_sigmoid).astype(jnp.bfloat16)
-    grad_mixed = jnp.dot(full_grad, out_proj, preferred_element_type=jnp.float32)
-    grad_normed = grad_mixed * norm_sigmoid * (1.0 + normed * (1.0 - norm_sigmoid))
-    first_sum, second_sum = packed_total(
-        (jnp.sum(grad_normed, axis=1), jnp.sum(grad_normed * normed, axis=1)), "tp"
-    )
-    grad_conv = inv_std * (
-        grad_normed - (first_sum / CW)[:, None] - normed * (second_sum / CW)[:, None]
-    )
-    kernel_width = conv_taps.shape[0]
-    rim_rows = passed_along(grad_conv[: kernel_width - 1], "sp", -1)
-    padded = jnp.concatenate([grad_conv, rim_rows], axis=0)
-    grad_glu = jnp.zeros_like(grad_conv)
-    for offset in range(kernel_width):
-        grad_glu = grad_glu + conv_taps[offset][None, :] * padded[offset : offset + tok_count]
-    gate_sig = jax.nn.sigmoid(glu_gate.astype(jnp.float32))
-    grad_value = (grad_glu * gate_sig).astype(jnp.bfloat16)
-    grad_gate = (grad_glu * glu_value.astype(jnp.float32) * gate_sig * (1.0 - gate_sig)).astype(
-        jnp.bfloat16
-    )
-    grad_out_proj = sum_at_owner(contract_rows(full_grad, mixed), "sp", 0)
     return (
         grad_stream,
-        grad_value,
-        grad_gate,
+        grad_value.T,
+        grad_gate.T,
         grad_out_proj,
-        grad_gate_w[None],
-        grad_up_w[None],
+        grad_gate_w.reshape(1, N_TP * SL, SL),
+        grad_up_w.reshape(1, N_TP * SL, SL),
         grad_down_w[None],
     )
 

time: 169 us -> 126 us (0.75)
  waiting for transfers between devices: 30.1 us -> 0 us
  starting transfers between devices: 22.5 us -> 0 us
  Pallas kernels: 92.4 us -> 112 us
  other arithmetic: 5.9 us -> 0 us
  local copies, waits for them, and re-layouts: 16.2 us -> 12.6 us
    all_to_all x4 -> x0, waiting for transfers between devices: 26.4 us -> none  [the longest x3 17.7 us: copy_for_each(): lax.all_to_all(jnp.broadcast_to(shard[None], (size, *shard.shape)), axis,...]
    all_to_all x4 -> x0, starting transfers between devices: 21 us -> none  [the longest x3 17.1 us: copy_for_each(): lax.all_to_all(jnp.broadcast_to(shard[None], (size, *shard.shape)), axis,...]
    pallas_call x1, Pallas kernels: 92.4 us -> 112 us  [main_call(): pl.pallas_call(main_kernel, out_shape=(jax.ShapeDtypeStruct((TOK, SL), BF...]
    ppermute x1 -> x0, waiting for transfers between devices: 3.67 us -> none  [passed_along(): return lax.ppermute(shard, axis, pairs)]
    convert_element_type x2 -> x0, other arithmetic: 2.35 us -> none  [the longest x1 1.71 us: on_device(): (grad_glu * glu_value.astype(jnp.float32) * gate_sig * (1.0 - gate_sig))....]
    broadcast_in_dim x3 -> x0, local copies, waits for them, and re-layouts: 2.27 us -> none  [copy_for_each(): jnp.broadcast_to(shard[None], (size, *shard.shape))]
    all_to_all x1 -> x0, other arithmetic: 1.89 us -> none  [sum_at_owner(): lax.all_to_all(tiles, axis, split_axis=0, concat_axis=0, tiled=True)]
    unnamed x24 -> x11, local copies, waits for them, and re-layouts: 12.4 us -> 12.6 us
  transfers between devices with their start and end apart: 5 -> 0, of which waited for: 4 -> 0; matrix products, arithmetic and copies ran while one was open for 5% -> 0% of each run, Pallas kernels for 55% -> 0%
where the time goes in v2:
time: 126 us
  Pallas kernels  112 us (89%)
  local copies, waits for them, and re-layouts  12.6 us (10%)
    pallas_call x1, Pallas kernels, main_call(): pl.pallas_call(main_kernel, out_shape=(jax.ShapeDtypeStruct((TOK, SL), BF...  112 us
    unnamed x11, local copies, waits for them, and re-layouts  12.6 us

profile of v2, /device:TPU:1, one launch (start us, length us, event | category | flops | bytes accessed | tf_op | source)
XLA Modules:
  0.0 125.5 jit_solution(14015349767275640044)
XLA Ops:
  0.6 112.3 %routed_experts.1 = (bf16[256,256]{1,0:T(8,128)(2,1)}, bf16[64,256]{1,0:T(8,128)(2,1)}, bf16[64,256]{1,0:T(8,128)(2,1)}, f32[64,64]{1,0:T(8,128)}, f32[8,256,256...) custom-call(bf16[256,2048]{1,0:T(8,128)(2,1)} %up_hbm.1, bf16[256,2048]{1,0:T(8,128)(2,1)} %st_hbm.1, ...), custom_call_target="tpu_custom_call" | custom-call | flops 8589934592 | bytes 16777216 | tf_op jit(solution)/shard_map/routed_experts/pallas_call | solution.py:569
  113.0 1.6 %copy.26 = bf16[256,256]{1,0:T(8,128)(2,1)} copy(bf16[256,256]{1,0:T(8,128)(2,1)} %get-tuple-element.28) | data formatting | bytes 262144
  114.5 1.4 %copy.27 = bf16[256,64]{0,1:T(8,128)(2,1)} copy(bf16[256,64]{0,1:T(8,128)(2,1)} %bitcast.18) | data formatting | bytes 65536
  115.9 1.4 %copy.28 = bf16[256,64]{0,1:T(8,128)(2,1)} copy(bf16[256,64]{0,1:T(8,128)(2,1)} %bitcast.17) | data formatting | bytes 65536
  117.3 1.4 %copy.29 = f32[64,64]{1,0:T(8,128)} copy(f32[64,64]{1,0:T(8,128)} %get-tuple-element.31) | data formatting | bytes 32768
  118.7 0.0 copy-start.1
  118.7 3.2 %copy.30 = f32[1,2048,256]{2,1,0:T(8,128)} copy(f32[1,2048,256]{2,1,0:T(8,128)} %bitcast.16) | data formatting | bytes 4194304
  121.9 0.0 copy-done.1
  121.9 0.0 copy-start
  121.9 1.3 %copy.31 = f32[1,2048,256]{2,1,0:T(8,128)} copy(f32[1,2048,256]{2,1,0:T(8,128)S(1)} %bitcast.15) | data formatting | bytes 4194304
  123.2 1.0 copy-done
  124.2 1.3 %copy.32 = f32[1,256,2048]{2,1,0:T(8,128)} copy(f32[1,256,2048]{2,1,0:T(8,128)S(1)} %bitcast.14) | data formatting | bytes 4194304
Async XLA Ops:
  118.7 3.2 %copy-start.1 = (f32[8,256,256]{2,1,0:T(8,128)S(1)}, f32[8,256,256]{2,1,0:T(8,128)}, u32[]{:S(2)}) copy-start(f32[8,256,256]{2,1,0:T(8,128)} %get-tuple-element.19) | copy-start | bytes 6291460
  121.9 2.3 %copy-start = (f32[256,2048]{1,0:T(8,128)S(1)}, f32[256,2048]{1,0:T(8,128)}, u32[]{:S(2)}) copy-start(f32[256,2048]{1,0:T(8,128)} %get-tuple-element.20) | copy-start | bytes 6291460

commit v3 on v2

v3 whole, which is shorter than its diff:
```python
import jax
import jax.numpy as jnp
from jax import lax
from jax.experimental import pallas as pl
from jax.experimental.pallas import tpu as pltpu
from jax.sharding import PartitionSpec as P

MESH = pl.DeviceIdType.MESH
BF16 = jnp.bfloat16
F32 = jnp.float32

CW = 512
NZ, NX, NY = 8, 4, 4
N_SP = 32
N_TP = 8
CAP = 32
TOK = 256
SL = 256
CHUNKS = ((0, 4), (4, 8), (12, 8), (20, 8), (28, 4))
NC = len(CHUNKS)
MAX = 8 * CAP

clamp_limit = 7.0
glu_alpha = 1.702
norm_eps = 1e-05

OFFSETS = (
    ((0, 0), (1, 0), (7, 0), (0, 1))
    + ((0, 2), (0, 3), (1, 2), (7, 2), (2, 0), (6, 0), (2, 2), (6, 2))
    + tuple((dz, dx) for dz in (4, 5) for dx in range(4))
    + ((3, 0), (3, 1), (3, 2), (3, 3), (2, 1), (6, 1), (2, 3), (6, 3))
    + ((1, 1), (7, 1), (1, 3), (7, 3))
)
OWN = 0
G_SLOT = (0, 1, 6, 2, 3, 6, 4, 5, 6, 6, 6, 6, 6, 6)
CH = 64
KW = 31


def dot_tn(left, right):
    return lax.dot_general(left, right, (((0,), (0,)), ((), ())), preferred_element_type=F32)


def dot_nt(left, right):
    return lax.dot_general(left, right, (((1,), (1,)), ((), ())), preferred_element_type=F32)


def dot_nn(left, right):
    return lax.dot_general(left, right, (((1,), (0,)), ((), ())), preferred_element_type=F32)


def main_kernel(
    up_hbm, st_hbm, routes_hbm, weights_hbm, wg_hbm, wu_hbm, wd_hbm,
    value_hbm, gate_hbm, taps_hbm, conv_hbm, proj_hbm,
    gs_out, gv_out, gq_out, go_out, gg_out, gu_out, gd_out,
    gs_ref, gv_ref, gq_ref, go_ref, acc_g, acc_u, acc_d,
    up_v, st_v, routes_v, weights_v, wg, wu, wd, send, xs, onehot, part, part_in, comb, ring_in, relay,
    row_out, ret, ggp, gup, act,
    value_v, gate_v, taps_v, conv_all, proj_all, hh, hn, mix, stat,
    pm, pm_in, pm_out, pm_got, sums, sums_in, conv_grad, gt, gt_in, gt_out, gt_got,
    far_sem, load_sem, out_sem, a_snd, a_rcv, g_snd, g_rcv, r_snd, r_rcv, b_snd, b_rcv,
    e_snd, e_rcv, j_snd, j_rcv, k_snd, k_rcv, p_snd, p_rcv, s_snd, s_rcv, h_snd, h_rcv, o_snd, o_rcv, f_snd, f_rcv,
):
    sp = lax.axis_index("sp")
    tp = lax.axis_index("tp")
    z, x = sp // NX, sp % NX
    y, c = tp // 2, tp % 2
    fwd, bwd = ((y + 1) % NY) * 2 + c, ((y + 3) % NY) * 2 + c
    opp = ((y + 2) % NY) * 2 + c
    other = y * 2 + (1 - c)
    up_dev, down_dev, mate = (sp, fwd), (sp, bwd), (sp, other)
    oc = 1 - c
    fwd_o, bwd_o, opp_o = ((y + 1) % NY) * 2 + oc, ((y + 3) % NY) * 2 + oc, ((y + 2) % NY) * 2 + oc

    def sp_dev(p, sign):
        dz, dx = OFFSETS[p]
        if sign < 0:
            dz, dx = (NZ - dz) % NZ, (NX - dx) % NX
        return (((z + dz) % NZ) * NX + (x + dx) % NX, tp)

    def whole(ref, sem):
        pltpu.make_async_copy(ref, ref, sem).wait()

    chunk_of = [k for k, (_, count) in enumerate(CHUNKS) for _ in range(count)]
    column = pl.multiple_of(tp * SL, SL)
    quarter = pl.ds(pl.multiple_of(x * (CH // NX), CH // NX), CH // NX)
    loads = [
        pltpu.make_async_copy(st_hbm.at[:, pl.ds(column, SL)], st_v, load_sem.at[0]),
        pltpu.make_async_copy(up_hbm.at[:, pl.ds(column, SL)], up_v, load_sem.at[1]),
        pltpu.make_async_copy(routes_hbm, routes_v, load_sem.at[2]),
        pltpu.make_async_copy(weights_hbm, weights_v, load_sem.at[3]),
    ]
    late = [
        pltpu.make_async_copy(wg_hbm, wg, load_sem.at[4]),
        pltpu.make_async_copy(wu_hbm, wu, load_sem.at[5]),
    ]
    for j in range(N_TP):
        late.append(
            pltpu.make_async_copy(wd_hbm.at[:, pl.ds(j * SL, SL)], wd.at[j], load_sem.at[6])
        )
    tail_loads = [
        pltpu.make_async_copy(value_hbm, value_v, load_sem.at[7]),
        pltpu.make_async_copy(gate_hbm, gate_v, load_sem.at[8]),
        pltpu.make_async_copy(taps_hbm, taps_v, load_sem.at[9]),
        pltpu.make_async_copy(conv_hbm, conv_all.at[tp], load_sem.at[10]),
        pltpu.make_async_copy(
            proj_hbm.at[quarter, pl.ds(column, SL)], proj_all.at[tp, quarter], load_sem.at[11]
        ),
    ]
    for copy in loads + late + tail_loads:
        copy.start()

    barrier = pltpu.get_barrier_semaphore()
    peers = [(sp, (tp + r) % N_TP) for r in range(1, N_TP)]
    near = [p for p in range(N_SP) if p != OWN and OFFSETS[p][0] in (0, 1, NZ - 1)]
    for dev in [sp_dev(p, 1) for p in near] + peers:
        pl.semaphore_signal(barrier, inc=1, device_id=dev, device_id_type=MESH)
    owners = [(tp * NX + a, sp // NX) for a in range(NX)]
    above, below = (((z + 1) % NZ) * NX + x, tp), (((z + NZ - 1) % NZ) * NX + x, tp)

    for copy in loads:
        copy.wait()
    packed = jnp.concatenate(
        [routes_v[...].astype(F32), weights_v[...], jnp.zeros((4, TOK), F32)], axis=0
    ).T
    r0, r1 = packed[:, 0:1].astype(jnp.int32), packed[:, 1:2].astype(jnp.int32)
    experts = lax.broadcasted_iota(jnp.int32, (TOK, N_SP), 1)
    c0 = jnp.where(r0 == experts, 1.0, 0.0).astype(F32)
    c1 = jnp.where(r1 == experts, 1.0, 0.0).astype(F32)
    tri = jnp.where(
        lax.broadcasted_iota(jnp.int32, (TOK, TOK), 1) < lax.broadcasted_iota(jnp.int32, (TOK, TOK), 0),
        1.0, 0.0,
    ).astype(BF16)
    expert = lax.broadcasted_iota(jnp.int32, (8, N_SP), 1)
    offset_of = (((expert >> 2) - z) & (NZ - 1)) * NX + (((expert & 3) - x) & (NX - 1))
    first_slot = jnp.zeros((8, N_SP), F32)
    for p, (dz, dx) in enumerate(OFFSETS):
        first_slot = first_slot + jnp.where(offset_of == dz * NX + dx, float(p * CAP), 0.0)
    slots = dot_nn(tri, (c0 + c1).astype(BF16)) + first_slot[0:1, :]
    pos0 = jnp.sum(slots * c0, axis=1, keepdims=True).astype(jnp.int32)
    pos1 = jnp.sum(slots * c1, axis=1, keepdims=True).astype(jnp.int32)
    stream = st_v[...]
    ups = up_v[...].astype(F32)
    cot0 = (packed[:, 2:3] * ups).astype(BF16)
    cot1 = (packed[:, 3:4] * ups).astype(BF16)

    def a2a(p):
        return pltpu.make_async_remote_copy(
            src_ref=send.at[p],
            dst_ref=xs.at[:, tp, pl.ds(p * CAP, CAP), :],
            send_sem=a_snd,
            recv_sem=a_rcv.at[chunk_of[p]],
            device_id=sp_dev(p, 1),
            device_id_type=MESH,
        )

    conv_plan = ((tp, up_dev), (tp, down_dev), (tp, (sp, opp)), (tp, mate), (bwd, mate), (fwd, mate), (opp, mate))
    conv_arrives = (bwd, fwd, opp, other, bwd_o, fwd_o, opp_o)

    def conv_copy(kind, arriving=False):
        at, dev = conv_plan[kind]
        if arriving:
            at = conv_arrives[kind]
        return pltpu.make_async_remote_copy(
            src_ref=conv_hbm if kind < 4 else conv_all.at[at], dst_ref=conv_all.at[at],
            send_sem=e_snd, recv_sem=e_rcv.at[kind], device_id=dev, device_id_type=MESH,
        )

    def proj_copy(r):
        at = pl.multiple_of(((tp + r) % N_TP) * SL, SL)
        return pltpu.make_async_remote_copy(
            src_ref=proj_hbm.at[quarter, pl.ds(at, SL)], dst_ref=proj_all.at[tp, quarter],
            send_sem=j_snd, recv_sem=j_rcv, device_id=peers[r - 1], device_id_type=MESH,
        )

    def quarter_copy(d):
        return pltpu.make_async_remote_copy(
            src_ref=proj_all.at[:, quarter, :], dst_ref=proj_all.at[:, quarter, :],
            send_sem=k_snd, recv_sem=k_rcv,
            device_id=(z * NX + (x + d) % NX, tp), device_id_type=MESH,
        )

    def stage_s(k):
        start, count = CHUNKS[k]
        width = count * CAP
        lanes = lax.broadcasted_iota(jnp.int32, (TOK, width), 1) + start * CAP
        s0 = jnp.where(pos0 == lanes, 1.0, 0.0).astype(BF16)
        s1 = jnp.where(pos1 == lanes, 1.0, 0.0).astype(BF16)
        both = s0 + s1
        onehot[:, start * CAP:start * CAP + width] = both
        rows = dot_tn(both, stream).astype(BF16)
        cots = (dot_tn(s0, cot0) + dot_tn(s1, cot1)).astype(BF16)
        send[start:start + count, 0] = rows.reshape(count, CAP, SL)
        send[start:start + count, 1] = cots.reshape(count, CAP, SL)

    def stage_go(k):
        start, count = CHUNKS[k]
        for p in range(start, start + count):
            if p == OWN:
                xs[:, tp, pl.ds(p * CAP, CAP), :] = send[p]
            else:
                a2a(p).start()

    def farther(step):
        for dev in (above, below):
            pl.semaphore_signal(far_sem.at[step], inc=1, device_id=dev, device_id_type=MESH)

    def stage_f(step):
        pl.semaphore_wait(far_sem.at[step], 2)
        if step < 2:
            farther(step + 1)

    stage_s(0)
    pl.semaphore_wait(barrier, len(near) + N_TP - 1)
    farther(0)
    stage_go(0)
    for kind in range(4):
        conv_copy(kind).start()
    for r in range(1, N_TP):
        proj_copy(r).start()
    stage_s(1)
    stage_f(0)
    stage_go(1)
    stage_s(2)
    stage_f(1)
    stage_s(3)
    stage_f(2)
    stage_s(4)

    def gather(k, kind, rc, slice_at, dev):
        start, count = CHUNKS[k]
        ref = xs.at[rc, slice_at, pl.ds(start * CAP, count * CAP), :]
        return pltpu.make_async_remote_copy(
            src_ref=ref, dst_ref=ref, send_sem=g_snd, recv_sem=g_rcv.at[k, G_SLOT[kind]],
            device_id=dev, device_id_type=MESH,
        )

    plan = (
        (0, tp, up_dev), (0, tp, down_dev), (0, tp, mate),
        (1, tp, up_dev), (1, tp, down_dev), (1, tp, mate),
        (0, bwd, up_dev), (1, fwd, down_dev),
        (0, bwd, mate), (0, fwd, mate), (0, opp, mate),
        (1, fwd, mate), (1, bwd, mate), (1, opp, mate),
    )

    def spread(k, kind):
        rc, slice_at, dev = plan[kind]
        return gather(k, kind, rc, slice_at, dev)

    arrives = (bwd, fwd, other, bwd, fwd, other, opp, opp, bwd_o, fwd_o, opp_o, fwd_o, bwd_o, opp_o)
    arrives_rc = (0, 0, 0, 1, 1, 1, 0, 1, 0, 0, 0, 1, 1, 1)

    def got(k, kind):
        gather(k, kind, arrives_rc[kind], arrives[kind], mate).wait_recv()

    def stage_a(k):
        start, count = CHUNKS[k]
        begin = max(start, 1)
        whole(xs.at[:, tp, pl.ds(begin * CAP, (start + count - begin) * CAP), :], a_rcv.at[k])
        for kind in (0, 4, 3, 1, 2, 5):
            spread(k, kind).start()

    def stage_b1(k):
        got(k, 0)
        spread(k, 6).start()
        got(k, 4)
        spread(k, 7).start()
        spread(k, 8).start()
        spread(k, 11).start()

    def stage_b2(k):
        got(k, 1)
        spread(k, 9).start()
        got(k, 3)
        spread(k, 12).start()
        got(k, 6)
        spread(k, 10).start()
        got(k, 7)
        spread(k, 13).start()

    def stage_b3(k):
        start, count = CHUNKS[k]
        whole(xs.at[:, pl.ds(0, NY), pl.ds(start * CAP, count * CAP), :], g_rcv.at[k, 6])

    def swap(k):
        return pltpu.make_async_remote_copy(
            src_ref=part.at[k, 1 - c, :, pl.ds(0, CHUNKS[k][1] * CAP), :],
            dst_ref=part_in.at[k, :, pl.ds(0, CHUNKS[k][1] * CAP), :],
            send_sem=r_snd, recv_sem=r_rcv.at[k, 0], device_id=mate, device_id_type=MESH,
        )

    def stage_c(k):
        start, count = CHUNKS[k]
        size = count * CAP
        rows = pl.ds(start * CAP, size)
        gate_pre = jnp.zeros((size, SL), F32)
        up_pre = jnp.zeros((size, SL), F32)
        grad_act = jnp.zeros((size, SL), F32)
        for j in range(N_TP):
            r = xs[0, j, rows, :]
            gate_pre = gate_pre + dot_nn(r, wg[j])
            up_pre = up_pre + dot_nn(r, wu[j])
            grad_act = grad_act + dot_nt(xs[1, j, rows, :], wd[j])
        capped = jnp.minimum(gate_pre, clamp_limit)
        clipped = jnp.clip(up_pre, -clamp_limit, clamp_limit)
        sig = jax.nn.sigmoid(glu_alpha * capped)
        act[rows, :] = (capped * sig * (clipped + 1.0)).astype(BF16)
        slope = sig + glu_alpha * capped * sig * (1.0 - sig)
        g_gate = jnp.where(gate_pre < clamp_limit, grad_act * (clipped + 1.0) * slope, 0.0).astype(BF16)
        g_up = jnp.where(jnp.abs(up_pre) < clamp_limit, grad_act * capped * sig, 0.0).astype(BF16)
        ggp[rows, :] = g_gate
        gup[rows, :] = g_up
        for j in range(N_TP):
            total = dot_nt(g_gate, wg[j]) + dot_nt(g_up, wu[j])
            part[k, j % 2, j // 2, 0:size] = total.astype(BF16)
        swap(k).start()

    def stage_w(start, stop):
        rows = pl.ds(start, stop - start)

        def grads(j, carry):
            r = xs[0, j, rows, :]
            at = pl.ds(pl.multiple_of(j * SL, SL), SL)
            g, u = dot_tn(r, ggp[rows, :]), dot_tn(r, gup[rows, :])
            d = dot_tn(act[rows, :], xs[1, j, rows, :])
            if start == 0:
                acc_g[j], acc_u[j], acc_d[:, at] = g, u, d
            else:
                acc_g[j] += g
                acc_u[j] += u
                acc_d[:, at] += d
            return carry

        lax.fori_loop(0, N_TP, grads, 0)

    def halves(k):
        half = CHUNKS[k][1] * CAP // 2
        return pl.ds(0, half), pl.ds(half, half)

    def ring(k, kind, src, slot, dev):
        return pltpu.make_async_remote_copy(
            src_ref=src, dst_ref=ring_in.at[k, slot, halves(k)[0], :],
            send_sem=r_snd, recv_sem=r_rcv.at[k, kind], device_id=dev, device_id_type=MESH,
        )

    def rings(k, kind):
        lo, hi = halves(k)
        if kind == 0:
            return swap(k)
        if kind == 1:
            return ring(k, 1, comb.at[k, 2, lo, :], 0, down_dev)
        if kind == 2:
            return ring(k, 2, comb.at[k, 2, hi, :], 1, up_dev)
        if kind == 3:
            return ring(k, 3, comb.at[k, 1, lo, :], 2, up_dev)
        if kind == 4:
            return ring(k, 4, comb.at[k, 3, hi, :], 3, down_dev)
        if kind == 5:
            return ring(k, 5, relay.at[k, 0, lo, :], 4, down_dev)
        return ring(k, 6, relay.at[k, 1, lo, :], 5, up_dev)

    def stage_d(k):
        rings(k, 0).wait_recv()
        size = CHUNKS[k][1] * CAP
        for r in (2, 1, 3, 0):
            at = (y + r) % NY
            both = part[k, c, at, 0:size].astype(F32) + part_in[k, at, 0:size].astype(F32)
            comb[k, r, 0:size] = both.astype(BF16)
            if r == 2:
                rings(k, 1).start()
                rings(k, 2).start()
        rings(k, 3).start()
        rings(k, 4).start()

    def stage_e1(k):
        rings(k, 1).wait_recv()
        lo, hi = halves(k)
        relay[k, 0, lo, :] = (ring_in[k, 0, lo, :].astype(F32) + comb[k, 3, lo, :].astype(F32)).astype(BF16)
        rings(k, 5).start()
        rings(k, 2).wait_recv()
        relay[k, 1, lo, :] = (ring_in[k, 1, lo, :].astype(F32) + comb[k, 1, hi, :].astype(F32)).astype(BF16)
        rings(k, 6).start()

    def back_copy(p):
        return pltpu.make_async_remote_copy(
            src_ref=row_out.at[p], dst_ref=ret.at[p],
            send_sem=b_snd, recv_sem=b_rcv.at[chunk_of[p]], device_id=sp_dev(p, -1), device_id_type=MESH,
        )

    def stage_e2(k):
        for kind in (3, 4, 5, 6):
            rings(k, kind).wait_recv()
        lo, hi = halves(k)
        low = comb[k, 0, lo, :].astype(F32) + ring_in[k, 2, lo, :].astype(F32) + ring_in[k, 4, lo, :].astype(F32)
        high = comb[k, 0, hi, :].astype(F32) + ring_in[k, 3, lo, :].astype(F32) + ring_in[k, 5, lo, :].astype(F32)
        at, count = CHUNKS[k]
        row_out[at:at + count // 2] = low.astype(BF16).reshape(count // 2, CAP, SL)
        row_out[at + count // 2:at + count] = high.astype(BF16).reshape(count // 2, CAP, SL)
        for p in range(at, at + count):
            if p == OWN:
                ret[p] = row_out[p]
            else:
                back_copy(p).start()

    def stage_m():
        for copy in tail_loads:
            copy.wait()
        for kind in range(3):
            conv_copy(kind, True).wait_recv()
            conv_copy(kind + 4).start()
        whole(proj_all.at[pl.ds(0, N_TP - 1), pl.ds(0, CH // NX), :], j_rcv)
        for d in range(1, NX):
            quarter_copy(d).start()

    def stage_n():
        for kind in range(3, 7):
            conv_copy(kind, True).wait_recv()
        total, square = jnp.zeros((1, TOK), F32), jnp.zeros((1, TOK), F32)
        for k in range(N_TP):
            v = conv_all[k].astype(F32)
            total = total + jnp.sum(v, axis=0, keepdims=True)
            square = square + jnp.sum(v * v, axis=0, keepdims=True)
        mean = total / CW
        inv = lax.rsqrt(square / CW - mean * mean + norm_eps)
        stat[0:1, :] = mean
        stat[1:2, :] = inv
        for k in range(N_TP):
            n = (conv_all[k].astype(F32) - mean) * inv
            sig = jax.nn.sigmoid(n)
            slope = sig * (1.0 + n * (1.0 - sig))
            mix[k] = (n * sig).astype(BF16)
            hh[k] = slope
            hn[k] = slope * n

    stage_a(0)
    stage_go(2)
    stage_b1(0)
    stage_a(1)
    stage_go(3)
    stage_go(4)
    stage_b2(0)
    late[0].wait()
    late[1].wait()
    whole(wd, load_sem.at[6])
    stage_b3(0)
    stage_c(0)
    stage_b1(1)
    stage_d(0)
    stage_a(2)
    stage_m()
    stage_b2(1)
    stage_e1(0)
    stage_b3(1)
    stage_c(1)
    stage_b1(2)
    stage_d(1)
    stage_a(3)
    stage_e2(0)
    stage_n()
    stage_b2(2)
    stage_e1(1)
    stage_b3(2)
    stage_c(2)
    stage_b1(3)
    stage_d(2)
    stage_a(4)
    stage_e2(1)
    stage_w(0, 384)
    stage_b2(3)
    stage_e1(2)
    stage_b3(3)
    stage_c(3)
    stage_b1(4)
    stage_d(3)
    stage_e2(2)
    stage_w(384, 640)
    stage_b2(4)
    stage_e1(3)
    stage_b3(4)
    stage_c(4)
    stage_e2(3)
    stage_d(4)
    stage_w(640, 896)
    stage_e1(4)
    stage_w(896, 1024)
    stage_e2(4)
    outs = [
        pltpu.make_async_copy(acc_g, gg_out, out_sem.at[4]),
        pltpu.make_async_copy(acc_u, gu_out, out_sem.at[5]),
        pltpu.make_async_copy(acc_d, gd_out, out_sem.at[6]),
    ]
    for copy in outs:
        copy.start()
    total = up_v[...].astype(F32)
    for start, count in CHUNKS:
        begin = max(start, 1)
        whole(ret.at[pl.ds(begin, start + count - begin)], b_rcv.at[chunk_of[start]])
        picked = onehot[:, start * CAP:(start + count) * CAP]
        total = total + dot_nn(picked, ret[start:start + count].reshape(count * CAP, SL))
    grads = total.astype(BF16)
    gs_ref[...] = grads

    whole(proj_all.at[:, pl.ds(0, 3 * CH // NX), :], k_rcv)
    prod = dot_nt(proj_all[...].reshape(CW, SL), grads)
    sums[0:1, :] = jnp.sum(prod * hh[...].reshape(CW, TOK), axis=0, keepdims=True)
    sums[1:2, :] = jnp.sum(prod * hn[...].reshape(CW, TOK), axis=0, keepdims=True)
    for k in range(N_TP):
        pm[k % 2, k // 2] = prod[k * CH:(k + 1) * CH].astype(BF16)

    def pm_copy(r):
        if r == 0:
            src, dst, dev = pm.at[1 - c], pm_in, mate
        else:
            src, dst, dev = pm_out.at[r - 1], pm_got.at[r - 1], (sp, ((y + r) % NY) * 2 + c)
        return pltpu.make_async_remote_copy(
            src_ref=src, dst_ref=dst, send_sem=p_snd, recv_sem=p_rcv.at[r],
            device_id=dev, device_id_type=MESH,
        )

    def sum_copy(r):
        return pltpu.make_async_remote_copy(
            src_ref=sums, dst_ref=sums_in.at[r - 1], send_sem=s_snd, recv_sem=s_rcv,
            device_id=peers[r - 1], device_id_type=MESH,
        )

    pm_copy(0).start()
    for r in range(1, N_TP):
        sum_copy(r).start()

    gt[...] = dot_nn(mix[...].reshape(CW, TOK), grads).astype(BF16).reshape(N_SP, CW // N_SP, SL)

    def gt_copy(p):
        dev = sp_dev(p, 1)
        return pltpu.make_async_remote_copy(
            src_ref=gt.at[dev[0]], dst_ref=gt_in.at[p], send_sem=o_snd, recv_sem=o_rcv,
            device_id=dev, device_id_type=MESH,
        )

    for p in range(N_SP):
        if p != OWN:
            gt_copy(p).start()

    pm_copy(0).wait_recv()
    for r in (2, 1, 3):
        at = (y + r) % NY
        pm_out[r - 1] = (pm[c, at].astype(F32) + pm_in[at].astype(F32)).astype(BF16)
        pm_copy(r).start()
    mixed_grad = pm[c, y].astype(F32) + pm_in[y].astype(F32)
    first, second = sums[0:1, :], sums[1:2, :]
    whole(sums_in, s_rcv)
    for r in range(1, N_TP):
        first = first + sums_in[r - 1, 0:1, :]
        second = second + sums_in[r - 1, 1:2, :]
    for r in (1, 3, 2):
        pm_copy(r).wait_recv()
        mixed_grad = mixed_grad + pm_got[r - 1].astype(F32)
    mean, inv = stat[0:1, :], stat[1:2, :]
    normed = (conv_all[tp].astype(F32) - mean) * inv
    grad_normed = mixed_grad * hh[tp]
    conv_grad[:, 0:TOK] = inv * (grad_normed - first / CW - normed * (second / CW))
    halo = pltpu.make_async_remote_copy(
        src_ref=conv_grad.at[:, pl.ds(0, 128)], dst_ref=conv_grad.at[:, pl.ds(TOK, 128)],
        send_sem=h_snd, recv_sem=h_rcv, device_id=((sp + N_SP - 1) % N_SP, tp), device_id_type=MESH,
    )
    halo.start()

    owned = gt[sp].astype(F32)
    whole(gt_in.at[pl.ds(1, N_SP - 1)], o_rcv)
    for p in range(N_SP):
        if p != OWN:
            owned = owned + gt_in[p].astype(F32)
    gt_out[0] = owned[:, 0:128]
    gt_out[1] = owned[:, 128:256]
    part_at = sp % NX

    def owner_copy(a, slot):
        return pltpu.make_async_remote_copy(
            src_ref=gt_out.at[a // 2], dst_ref=gt_got.at[slot], send_sem=f_snd.at[a], recv_sem=f_rcv.at[slot],
            device_id=owners[a], device_id_type=MESH,
        )

    for a in range(NX):
        mine = (sp // NX == tp) & (part_at == a)

        @pl.when(mine)
        def _(a=a):
            gt_got[a] = gt_out[a // 2]

        @pl.when(jnp.logical_not(mine))
        def _(a=a):
            owner_copy(a, part_at).start()

    halo.wait_recv()
    tail = conv_grad[:, TOK:TOK + 128]
    wide = jnp.concatenate([conv_grad[:, 0:TOK], jnp.where(sp == N_SP - 1, 0.0, tail)], axis=1)
    taps_t = jnp.concatenate([taps_v[...], jnp.zeros((1, CH), F32)], axis=0).T
    glu = taps_t[:, 0:1] * wide[:, 0:TOK]
    for offset in range(1, KW):
        glu = glu + taps_t[:, offset:offset + 1] * pltpu.roll(wide, TOK + 128 - offset, 1)[:, 0:TOK]
    gate_sig = jax.nn.sigmoid(gate_v[...].astype(F32))
    gv_ref[...] = (glu * gate_sig).astype(BF16)
    gq_ref[...] = (glu * value_v[...].astype(F32) * gate_sig * (1.0 - gate_sig)).astype(BF16)

    for a in range(NX):
        mine = (sp // NX == tp) & (part_at == a)

        @pl.when(jnp.logical_not(mine))
        def _(a=a):
            owner_copy(a, a).wait_recv()
            owner_copy(a, part_at).wait_send()

    got_t = gt_got[...].reshape(CH, 128).T
    go_ref[...] = jnp.where(part_at % 2 == 0, got_t[0:CH, :], got_t[CH:2 * CH, :])

    outs.extend([
        pltpu.make_async_copy(gs_ref, gs_out, out_sem.at[0]),
        pltpu.make_async_copy(gv_ref, gv_out, out_sem.at[1]),
        pltpu.make_async_copy(gq_ref, gq_out, out_sem.at[2]),
        pltpu.make_async_copy(go_ref, go_out, out_sem.at[3]),
    ])
    for copy in outs[3:]:
        copy.start()
    whole(send.at[pl.ds(1, N_SP - 1)], a_snd)
    whole(row_out.at[pl.ds(1, N_SP - 1)], b_snd)
    whole(gt_in.at[pl.ds(1, N_SP - 1)], o_snd)
    whole(xs.at[:, pl.ds(0, 7)], g_snd)
    whole(xs.at[0, pl.ds(0, 7)], r_snd)
    whole(conv_all.at[pl.ds(0, 7)], p_snd)
    whole(sums_in, s_snd)
    whole(proj_all.at[pl.ds(0, N_TP - 1), pl.ds(0, CH // NX), :], j_snd)
    whole(proj_all.at[:, pl.ds(0, 3 * CH // NX), :], k_snd)
    whole(conv_all.at[pl.ds(0, 7)], e_snd)
    for copy in outs:
        copy.wait()
    halo.wait_send()


RESULTS = (
    ((TOK, SL), BF16),
    ((CH, TOK), BF16),
    ((CH, TOK), BF16),
    ((CH, CH), F32),
    ((N_TP, SL, SL), F32),
    ((N_TP, SL, SL), F32),
    ((SL, N_TP * SL), F32),
)


def store_kernel(*refs):
    n = len(RESULTS)
    sems = refs[-1]
    copies = [pltpu.make_async_copy(refs[i], refs[n + i], sems.at[i]) for i in range(n)]
    for copy in copies:
        copy.start()
    for copy in copies:
        copy.wait()


def store_call(*results):
    return pl.pallas_call(
        store_kernel,
        out_shape=tuple(jax.ShapeDtypeStruct(shape, dtype) for shape, dtype in RESULTS),
        in_specs=[pl.BlockSpec(memory_space=pltpu.VMEM)] * len(RESULTS),
        out_specs=(pl.BlockSpec(memory_space=pl.ANY),) * len(RESULTS),
        scratch_shapes=[pltpu.SemaphoreType.DMA((len(RESULTS),))],
        compiler_params=pltpu.CompilerParams(vmem_limit_bytes=2 * 1024 * 1024),
        name="store_results",
    )(*(pltpu.with_memory_space_constraint(r, pltpu.VMEM) for r in results))


def main_call(*operands):
    any_spec = pl.BlockSpec(memory_space=pltpu.HBM)
    flops = 2 * N_SP * CAP * 2048 * 256 * 8
    V = pltpu.VMEM
    D = pltpu.SemaphoreType.DMA
    return pl.pallas_call(
        main_kernel,
        out_shape=tuple(V(shape, dtype) for shape, dtype in RESULTS),
        in_specs=[any_spec] * 12,
        out_specs=(pl.BlockSpec(memory_space=pl.ANY),) * 7,
        scratch_shapes=[V(shape, dtype) for shape, dtype in RESULTS] + [
            V((TOK, SL), BF16),
            V((TOK, SL), BF16),
            V((2, TOK), jnp.int32),
            V((2, TOK), F32),
            V((N_TP, SL, SL), BF16),
            V((N_TP, SL, SL), BF16),
            V((N_TP, SL, SL), BF16),
            V((N_SP, 2, CAP, SL), BF16),
            V((2, N_TP, N_SP * CAP, SL), BF16),
            V((TOK, N_SP * CAP), BF16),
            V((NC, 2, NY, MAX, SL), BF16),
            V((NC, NY, MAX, SL), BF16),
            V((NC, NY, MAX, SL), BF16),
            V((NC, 6, MAX // 2, SL), BF16),
            V((NC, 2, MAX // 2, SL), BF16),
            V((N_SP, CAP, SL), BF16),
            V((N_SP, CAP, SL), BF16),
            V((N_SP * CAP, SL), BF16),
            V((N_SP * CAP, SL), BF16),
            V((N_SP * CAP, SL), BF16),
            V((CH, TOK), BF16),
            V((CH, TOK), BF16),
            V((KW, CH), F32),
            V((N_TP, CH, TOK), BF16),
            V((N_TP, CH, SL), BF16),
            V((N_TP, CH, TOK), F32),
            V((N_TP, CH, TOK), F32),
            V((N_TP, CH, TOK), BF16),
            V((8, TOK), F32),
            V((2, NY, CH, TOK), BF16),
            V((NY, CH, TOK), BF16),
            V((NY - 1, CH, TOK), BF16),
            V((NY - 1, CH, TOK), BF16),
            V((8, TOK), F32),
            V((N_TP - 1, 8, TOK), F32),
            V((CH, TOK + 128), F32),
            V((N_SP, CW // N_SP, SL), BF16),
            V((N_SP, CW // N_SP, SL), BF16),
            V((2, CW // N_SP, 128), F32),
            V((NX, CW // N_SP, 128), F32),
            pltpu.SemaphoreType.REGULAR((3,)),
            D((12,)),
            D((7,)),
            D,
            D((NC,)),
            D,
            D((NC, 7)),
            D,
            D((NC, 7)),
            D,
            D((NC,)),
            D,
            D((7,)),
            D,
            D,
            D,
            D,
            D,
            D((NY,)),
            D,
            D,
            D,
            D,
            D,
            D,
            D((NX,)),
            D((NX,)),
        ],
        compiler_params=pltpu.CompilerParams(
            collective_id=0, has_side_effects=True, vmem_limit_bytes=54 * 1024 * 1024
        ),
        cost_estimate=pl.CostEstimate(flops=flops, bytes_accessed=16 << 20, transcendentals=0),
        name="routed_experts",
    )(*operands)


def on_device(
    upstream,
    stream,
    routes,
    route_weights,
    glu_value,
    glu_gate,
    conv_taps,
    conv_saved,
    out_proj,
    expert_gate,
    expert_up,
    expert_down,
):
    grad_stream, grad_value, grad_gate, grad_out_proj, grad_gate_w, grad_up_w, grad_down_w = store_call(*main_call(
        upstream, stream, routes.T, route_weights.T,
        expert_gate.reshape(N_TP, SL, SL), expert_up.reshape(N_TP, SL, SL), expert_down[0],
        glu_value.T, glu_gate.T, conv_taps, conv_saved.T, out_proj.T,
    ))
    return (
        grad_stream,
        grad_value.T,
        grad_gate.T,
        grad_out_proj,
        grad_gate_w.reshape(1, N_TP * SL, SL),
        grad_up_w.reshape(1, N_TP * SL, SL),
        grad_down_w[None],
    )


def solution(mesh):
    in_specs = (
        P("sp", None),
        P("sp", None),
        P("sp", None),
        P("sp", None),
        P("sp", "tp"),
        P("sp", "tp"),
        P(None, "tp"),
        P("sp", "tp"),
        P(None, "tp"),
        P("sp", None, "tp"),
        P("sp", None, "tp"),
        P("sp", "tp", None),
    )
    out_specs = (
        P("sp", "tp"),
        P("sp", "tp"),
        P("sp", "tp"),
        P("sp", "tp"),
        P("sp", None, "tp"),
        P("sp", None, "tp"),
        P("sp", "tp", None),
    )
    return jax.shard_map(
        on_device, mesh=mesh, in_specs=in_specs, out_specs=out_specs, check_vma=False
    )
```

time: 126 us -> 104 us (0.83)
  local copies, waits for them, and re-layouts: 12.6 us -> 0 us
  Pallas kernels: 112 us -> 103 us
    unnamed x11 -> x0, local copies, waits for them, and re-layouts: 12.6 us -> none
    pallas_call x1 -> x2, Pallas kernels: 112 us -> 103 us  [the longest x1 100 us: main_call(): pl.pallas_call(main_kernel, out_shape=tuple((V(shape, dtype) for shape, d...]
where the time goes in v3:
time: 104 us
  Pallas kernels  103 us (99%)
    pallas_call x1, Pallas kernels, main_call(): pl.pallas_call(main_kernel, out_shape=tuple((V(shape, dtype) for shape, d...  100 us
    pallas_call x1, Pallas kernels, store_call(): pl.pallas_call(store_kernel, out_shape=tuple((jax.ShapeDtypeStruct(shape,...  2.84 us

profile of v3, /device:TPU:1, one launch (start us, length us, event | category | flops | bytes accessed | tf_op | source)
XLA Modules:
  0.0 103.8 jit_solution(13854832455935253437)
XLA Ops:
  0.6 100.2 %routed_experts.1 = (bf16[256,256]{1,0:T(8,128)(2,1)S(1)}, bf16[64,256]{1,0:T(8,128)(2,1)S(1)}, bf16[64,256]{1,0:T(8,128)(2,1)S(1)}, f32[64,64]{1,0:T(8,128)S(1)...) custom-call(bf16[256,2048]{1,0:T(8,128)(2,1)} %up_hbm.1, ...), custom_call_target="tpu_custom_call" | custom-call | flops 8589934592 | bytes 16777216 | tf_op jit(solution)/shard_map/routed_experts/pallas_call | solution.py:676
  100.8 2.8 %store_results.1 = (bf16[256,256]{1,0:T(8,128)(2,1)}, bf16[64,256]{1,0:T(8,128)(2,1)}, bf16[64,256]{1,0:T(8,128)(2,1)}, f32[64,64]{1,0:T(8,128)}, f32[8,256,256]...) custom-call(bf16[256,256]{1,0:T(8,128)(2,1)S(1)} %get-tuple-element.21.refs_0_, ...), custom_call_target="tpu_custom_call" | custom-call | tf_op jit(solution)/shard_map/store_results/pallas_call | solution.py:660

commit v4 on v3

--- a/solution.py
+++ b/solution.py
@@ -26,12 +26,21 @@
 
 OFFSETS = (
     ((0, 0), (1, 0), (7, 0), (0, 1))
-    + ((0, 2), (0, 3), (1, 2), (7, 2), (2, 0), (6, 0), (2, 2), (6, 2))
-    + tuple((dz, dx) for dz in (4, 5) for dx in range(4))
-    + ((3, 0), (3, 1), (3, 2), (3, 3), (2, 1), (6, 1), (2, 3), (6, 3))
-    + ((1, 1), (7, 1), (1, 3), (7, 3))
+    + ((0, 3), (0, 2), (1, 1), (7, 1), (1, 3), (7, 3), (2, 0), (6, 0))
+    + ((3, 0), (5, 0), (3, 1), (5, 1), (3, 2), (5, 2), (3, 3), (5, 3))
+    + ((4, 0), (4, 1), (4, 2), (4, 3), (1, 2), (7, 2), (2, 2), (6, 2))
+    + ((2, 1), (6, 1), (2, 3), (6, 3))
 )
+DIRECT = (0, 4)
+SECOND = {p: i for i, p in enumerate(p for k in DIRECT for p in range(CHUNKS[k][0], sum(CHUNKS[k])))}
 OWN = 0
+
+
+def far_first(positions):
+    hops = lambda p: min(OFFSETS[p][0], 8 - OFFSETS[p][0]) + min(OFFSETS[p][1], 4 - OFFSETS[p][1])
+    return sorted(positions, key=lambda p: (-hops(p), p))
+
+
 G_SLOT = (0, 1, 6, 2, 3, 6, 4, 5, 6, 6, 6, 6, 6, 6)
 CH = 64
 KW = 31
@@ -54,7 +63,7 @@
     value_hbm, gate_hbm, taps_hbm, conv_hbm, proj_hbm,
     gs_out, gv_out, gq_out, go_out, gg_out, gu_out, gd_out,
     gs_ref, gv_ref, gq_ref, go_ref, acc_g, acc_u, acc_d,
-    up_v, st_v, routes_v, weights_v, wg, wu, wd, send, xs, onehot, part, part_in, comb, ring_in, relay,
+    up_v, st_v, up_o, st_o, routes_v, weights_v, wg, wu, wd, send, send_o, xs, onehot, part, part_in, comb, ring_in, relay,
     row_out, ret, ggp, gup, act,
     value_v, gate_v, taps_v, conv_all, proj_all, hh, hn, mix, stat,
     pm, pm_in, pm_out, pm_got, sums, sums_in, conv_grad, gt, gt_in, gt_out, gt_got,
@@ -83,10 +92,13 @@
 
     chunk_of = [k for k, (_, count) in enumerate(CHUNKS) for _ in range(count)]
     column = pl.multiple_of(tp * SL, SL)
+    column_o = pl.multiple_of(opp * SL, SL)
     quarter = pl.ds(pl.multiple_of(x * (CH // NX), CH // NX), CH // NX)
     loads = [
         pltpu.make_async_copy(st_hbm.at[:, pl.ds(column, SL)], st_v, load_sem.at[0]),
         pltpu.make_async_copy(up_hbm.at[:, pl.ds(column, SL)], up_v, load_sem.at[1]),
+        pltpu.make_async_copy(st_hbm.at[:, pl.ds(column_o, SL)], st_o, load_sem.at[12]),
+        pltpu.make_async_copy(up_hbm.at[:, pl.ds(column_o, SL)], up_o, load_sem.at[13]),
         pltpu.make_async_copy(routes_hbm, routes_v, load_sem.at[2]),
         pltpu.make_async_copy(weights_hbm, weights_v, load_sem.at[3]),
     ]
@@ -107,15 +119,15 @@
             proj_hbm.at[quarter, pl.ds(column, SL)], proj_all.at[tp, quarter], load_sem.at[11]
         ),
     ]
-    for copy in loads + late + tail_loads:
-        copy.start()
-
     barrier = pltpu.get_barrier_semaphore()
     peers = [(sp, (tp + r) % N_TP) for r in range(1, N_TP)]
     near = [p for p in range(N_SP) if p != OWN and OFFSETS[p][0] in (0, 1, NZ - 1)]
     for dev in [sp_dev(p, 1) for p in near] + peers:
         pl.semaphore_signal(barrier, inc=1, device_id=dev, device_id_type=MESH)
-    owners = [(tp * NX + a, sp // NX) for a in range(NX)]
+    for copy in loads:
+        copy.start()
+    for copy in late + tail_loads:
+        copy.start()
     above, below = (((z + 1) % NZ) * NX + x, tp), (((z + NZ - 1) % NZ) * NX + x, tp)
 
     for copy in loads:
@@ -143,12 +155,26 @@
     ups = up_v[...].astype(F32)
     cot0 = (packed[:, 2:3] * ups).astype(BF16)
     cot1 = (packed[:, 3:4] * ups).astype(BF16)
+    stream_o = st_o[...]
+    ups_o = up_o[...].astype(F32)
+    cot0_o = (packed[:, 2:3] * ups_o).astype(BF16)
+    cot1_o = (packed[:, 3:4] * ups_o).astype(BF16)
 
     def a2a(p):
         return pltpu.make_async_remote_copy(
             src_ref=send.at[p],
             dst_ref=xs.at[:, tp, pl.ds(p * CAP, CAP), :],
-            send_sem=a_snd,
+            send_sem=a_snd.at[0],
+            recv_sem=a_rcv.at[chunk_of[p]],
+            device_id=sp_dev(p, 1),
+            device_id_type=MESH,
+        )
+
+    def a2a_o(p):
+        return pltpu.make_async_remote_copy(
+            src_ref=send_o.at[SECOND[p]],
+            dst_ref=xs.at[:, opp, pl.ds(p * CAP, CAP), :],
+            send_sem=a_snd.at[1],
             recv_sem=a_rcv.at[chunk_of[p]],
             device_id=sp_dev(p, 1),
             device_id_type=MESH,
@@ -192,14 +218,23 @@
         cots = (dot_tn(s0, cot0) + dot_tn(s1, cot1)).astype(BF16)
         send[start:start + count, 0] = rows.reshape(count, CAP, SL)
         send[start:start + count, 1] = cots.reshape(count, CAP, SL)
+        if k in DIRECT:
+            at = SECOND[start]
+            rows = dot_tn(both, stream_o).astype(BF16)
+            cots = (dot_tn(s0, cot0_o) + dot_tn(s1, cot1_o)).astype(BF16)
+            send_o[at:at + count, 0] = rows.reshape(count, CAP, SL)
+            send_o[at:at + count, 1] = cots.reshape(count, CAP, SL)
 
     def stage_go(k):
         start, count = CHUNKS[k]
         for p in range(start, start + count):
             if p == OWN:
                 xs[:, tp, pl.ds(p * CAP, CAP), :] = send[p]
+                xs[:, opp, pl.ds(p * CAP, CAP), :] = send_o[SECOND[p]]
             else:
                 a2a(p).start()
+                if k in DIRECT:
+                    a2a_o(p).start()
 
     def farther(step):
         for dev in (above, below):
@@ -211,6 +246,7 @@
             farther(step + 1)
 
     stage_s(0)
+    stage_s(1)
     pl.semaphore_wait(barrier, len(near) + N_TP - 1)
     farther(0)
     stage_go(0)
@@ -218,20 +254,17 @@
         conv_copy(kind).start()
     for r in range(1, N_TP):
         proj_copy(r).start()
-    stage_s(1)
     stage_f(0)
     stage_go(1)
     stage_s(2)
     stage_f(1)
-    stage_s(3)
-    stage_f(2)
-    stage_s(4)
+    stage_go(2)
 
     def gather(k, kind, rc, slice_at, dev):
         start, count = CHUNKS[k]
         ref = xs.at[rc, slice_at, pl.ds(start * CAP, count * CAP), :]
         return pltpu.make_async_remote_copy(
-            src_ref=ref, dst_ref=ref, send_sem=g_snd, recv_sem=g_rcv.at[k, G_SLOT[kind]],
+            src_ref=ref, dst_ref=ref, send_sem=g_snd.at[1 if k in DIRECT else 0], recv_sem=g_rcv.at[k, G_SLOT[kind]],
             device_id=dev, device_id_type=MESH,
         )
 
@@ -256,15 +289,18 @@
     def stage_a(k):
         start, count = CHUNKS[k]
         begin = max(start, 1)
-        whole(xs.at[:, tp, pl.ds(begin * CAP, (start + count - begin) * CAP), :], a_rcv.at[k])
-        for kind in (0, 4, 3, 1, 2, 5):
+        slices = 2 if k in DIRECT else 1
+        whole(xs.at[:, pl.ds(0, slices), pl.ds(begin * CAP, (start + count - begin) * CAP), :], a_rcv.at[k])
+        for kind in (0, 4, 3, 1, 2, 5) + ((10, 13) if k in DIRECT else ()):
             spread(k, kind).start()
 
     def stage_b1(k):
         got(k, 0)
-        spread(k, 6).start()
+        if k not in DIRECT:
+            spread(k, 6).start()
         got(k, 4)
-        spread(k, 7).start()
+        if k not in DIRECT:
+            spread(k, 7).start()
         spread(k, 8).start()
         spread(k, 11).start()
 
@@ -273,10 +309,11 @@
         spread(k, 9).start()
         got(k, 3)
         spread(k, 12).start()
-        got(k, 6)
-        spread(k, 10).start()
-        got(k, 7)
-        spread(k, 13).start()
+        if k not in DIRECT:
+            got(k, 6)
+            spread(k, 10).start()
+            got(k, 7)
+            spread(k, 13).start()
 
     def stage_b3(k):
         start, count = CHUNKS[k]
@@ -310,10 +347,12 @@
         g_up = jnp.where(jnp.abs(up_pre) < clamp_limit, grad_act * capped * sig, 0.0).astype(BF16)
         ggp[rows, :] = g_gate
         gup[rows, :] = g_up
-        for j in range(N_TP):
-            total = dot_nt(g_gate, wg[j]) + dot_nt(g_up, wu[j])
-            part[k, j % 2, j // 2, 0:size] = total.astype(BF16)
-        swap(k).start()
+        for i in range(N_TP):
+            core, at = (1 - c, i) if i < NY else (c, i - NY)
+            total = dot_nt(g_gate, wg[2 * at + core]) + dot_nt(g_up, wu[2 * at + core])
+            part[k, core, at, 0:size] = total.astype(BF16)
+            if i == NY - 1:
+                swap(k).start()
 
     def stage_w(start, stop):
         rows = pl.ds(start, stop - start)
@@ -340,7 +379,7 @@
     def ring(k, kind, src, slot, dev):
         return pltpu.make_async_remote_copy(
             src_ref=src, dst_ref=ring_in.at[k, slot, halves(k)[0], :],
-            send_sem=r_snd, recv_sem=r_rcv.at[k, kind], device_id=dev, device_id_type=MESH,
+            send_sem=r_snd, recv_sem=r_rcv.at[k, min(kind, 3)], device_id=dev, device_id_type=MESH,
         )
 
     def rings(k, kind):
@@ -388,15 +427,14 @@
         )
 
     def stage_e2(k):
-        for kind in (3, 4, 5, 6):
-            rings(k, kind).wait_recv()
         lo, hi = halves(k)
+        whole(ring_in.at[k, pl.ds(2, 4), lo, :], r_rcv.at[k, 3])
         low = comb[k, 0, lo, :].astype(F32) + ring_in[k, 2, lo, :].astype(F32) + ring_in[k, 4, lo, :].astype(F32)
         high = comb[k, 0, hi, :].astype(F32) + ring_in[k, 3, lo, :].astype(F32) + ring_in[k, 5, lo, :].astype(F32)
         at, count = CHUNKS[k]
         row_out[at:at + count // 2] = low.astype(BF16).reshape(count // 2, CAP, SL)
         row_out[at + count // 2:at + count] = high.astype(BF16).reshape(count // 2, CAP, SL)
-        for p in range(at, at + count):
+        for p in far_first(range(at, at + count)):
             if p == OWN:
                 ret[p] = row_out[p]
             else:
@@ -433,11 +471,13 @@
             hn[k] = slope * n
 
     stage_a(0)
-    stage_go(2)
-    stage_b1(0)
+    stage_s(3)
+    stage_f(2)
+    stage_s(4)
     stage_a(1)
     stage_go(3)
     stage_go(4)
+    stage_b1(0)
     stage_b2(0)
     late[0].wait()
     late[1].wait()
@@ -449,41 +489,41 @@
     stage_a(2)
     stage_m()
     stage_b2(1)
-    stage_e1(0)
     stage_b3(1)
     stage_c(1)
+    stage_e1(0)
     stage_b1(2)
     stage_d(1)
     stage_a(3)
     stage_e2(0)
     stage_n()
+    stage_w(0, 384)
     stage_b2(2)
-    stage_e1(1)
     stage_b3(2)
     stage_c(2)
+    stage_e1(1)
     stage_b1(3)
     stage_d(2)
     stage_a(4)
+    stage_w(384, 640)
     stage_e2(1)
-    stage_w(0, 384)
     stage_b2(3)
-    stage_e1(2)
     stage_b3(3)
     stage_c(3)
     stage_b1(4)
+    stage_e1(2)
     stage_d(3)
-    stage_e2(2)
-    stage_w(384, 640)
     stage_b2(4)
-    stage_e1(3)
     stage_b3(4)
     stage_c(4)
-    stage_e2(3)
+    stage_e2(2)
+    stage_e1(3)
     stage_d(4)
     stage_w(640, 896)
     stage_e1(4)
+    stage_e2(3)
+    stage_e2(4)
     stage_w(896, 1024)
-    stage_e2(4)
     outs = [
         pltpu.make_async_copy(acc_g, gg_out, out_sem.at[4]),
         pltpu.make_async_copy(acc_u, gu_out, out_sem.at[5]),
@@ -500,6 +540,26 @@
     grads = total.astype(BF16)
     gs_ref[...] = grads
 
+    outer = dot_nn(mix[...].reshape(CW, TOK), grads).reshape(N_TP, 2, CH // 2, SL)
+    low_half = lax.broadcasted_iota(jnp.int32, (CW // 2, 128), 1) < CH
+    for g in range(2):
+        upper = outer[:, 0, :, 128 * g:128 * g + 128].reshape(CW // 2, 128)
+        lower = outer[:, 1, :, 128 * g:128 * g + 128].reshape(CW // 2, 128)
+        even = jnp.where(low_half, upper, pltpu.roll(lower, CH, 1))
+        odd = jnp.where(low_half, pltpu.roll(upper, CH, 1), lower)
+        gt[:, 2 * g] = even.astype(BF16).reshape(N_TP, CH // 2, 128)
+        gt[:, 2 * g + 1] = odd.astype(BF16).reshape(N_TP, CH // 2, 128)
+    def gt_copy(p):
+        dev = sp_dev(p, 1)
+        return pltpu.make_async_remote_copy(
+            src_ref=gt.at[dev[0] // NX, dev[0] % NX], dst_ref=gt_in.at[p], send_sem=o_snd, recv_sem=o_rcv,
+            device_id=dev, device_id_type=MESH,
+        )
+
+    for p in far_first(range(N_SP)):
+        if p != OWN:
+            gt_copy(p).start()
+
     whole(proj_all.at[:, pl.ds(0, 3 * CH // NX), :], k_rcv)
     prod = dot_nt(proj_all[...].reshape(CW, SL), grads)
     sums[0:1, :] = jnp.sum(prod * hh[...].reshape(CW, TOK), axis=0, keepdims=True)
@@ -526,19 +586,6 @@
     pm_copy(0).start()
     for r in range(1, N_TP):
         sum_copy(r).start()
-
-    gt[...] = dot_nn(mix[...].reshape(CW, TOK), grads).astype(BF16).reshape(N_SP, CW // N_SP, SL)
-
-    def gt_copy(p):
-        dev = sp_dev(p, 1)
-        return pltpu.make_async_remote_copy(
-            src_ref=gt.at[dev[0]], dst_ref=gt_in.at[p], send_sem=o_snd, recv_sem=o_rcv,
-            device_id=dev, device_id_type=MESH,
-        )
-
-    for p in range(N_SP):
-        if p != OWN:
-            gt_copy(p).start()
 
     pm_copy(0).wait_recv()
     for r in (2, 1, 3):
@@ -564,31 +611,25 @@
     )
     halo.start()
 
-    owned = gt[sp].astype(F32)
     whole(gt_in.at[pl.ds(1, N_SP - 1)], o_rcv)
+    owned = gt[z, x].astype(F32)
     for p in range(N_SP):
         if p != OWN:
             owned = owned + gt_in[p].astype(F32)
-    gt_out[0] = owned[:, 0:128]
-    gt_out[1] = owned[:, 128:256]
-    part_at = sp % NX
-
-    def owner_copy(a, slot):
-        return pltpu.make_async_remote_copy(
-            src_ref=gt_out.at[a // 2], dst_ref=gt_got.at[slot], send_sem=f_snd.at[a], recv_sem=f_rcv.at[slot],
-            device_id=owners[a], device_id_type=MESH,
-        )
-
-    for a in range(NX):
-        mine = (sp // NX == tp) & (part_at == a)
-
-        @pl.when(mine)
-        def _(a=a):
-            gt_got[a] = gt_out[a // 2]
-
-        @pl.when(jnp.logical_not(mine))
-        def _(a=a):
-            owner_copy(a, part_at).start()
+    gt_out[...] = owned
+    here = z == tp
+    owner_copy = pltpu.make_async_remote_copy(
+        src_ref=gt_out, dst_ref=gt_got, send_sem=f_snd, recv_sem=f_rcv,
+        device_id=(tp * NX + x, z), device_id_type=MESH,
+    )
+
+    @pl.when(here)
+    def _():
+        gt_got[...] = gt_out[...]
+
+    @pl.when(jnp.logical_not(here))
+    def _():
+        owner_copy.start()
 
     halo.wait_recv()
     tail = conv_grad[:, TOK:TOK + 128]
@@ -601,17 +642,14 @@
     gv_ref[...] = (glu * gate_sig).astype(BF16)
     gq_ref[...] = (glu * value_v[...].astype(F32) * gate_sig * (1.0 - gate_sig)).astype(BF16)
 
-    for a in range(NX):
-        mine = (sp // NX == tp) & (part_at == a)
-
-        @pl.when(jnp.logical_not(mine))
-        def _(a=a):
-            owner_copy(a, a).wait_recv()
-            owner_copy(a, part_at).wait_send()
-
-    got_t = gt_got[...].reshape(CH, 128).T
-    go_ref[...] = jnp.where(part_at % 2 == 0, got_t[0:CH, :], got_t[CH:2 * CH, :])
-
+    @pl.when(jnp.logical_not(here))
+    def _():
+        owner_copy.wait_recv()
+        owner_copy.wait_send()
+
+    got_t = gt_got[...].T
+    go_ref[:, 0:CH // 2] = got_t[0:CH]
+    go_ref[:, CH // 2:CH] = got_t[CH:2 * CH]
     outs.extend([
         pltpu.make_async_copy(gs_ref, gs_out, out_sem.at[0]),
         pltpu.make_async_copy(gv_ref, gv_out, out_sem.at[1]),
@@ -620,10 +658,13 @@
     ])
     for copy in outs[3:]:
         copy.start()
-    whole(send.at[pl.ds(1, N_SP - 1)], a_snd)
+    whole(send.at[pl.ds(1, N_SP - 1)], a_snd.at[0])
+    whole(send_o.at[pl.ds(1, len(SECOND) - 1)], a_snd.at[1])
     whole(row_out.at[pl.ds(1, N_SP - 1)], b_snd)
     whole(gt_in.at[pl.ds(1, N_SP - 1)], o_snd)
-    whole(xs.at[:, pl.ds(0, 7)], g_snd)
+
+    whole(xs.at[:, pl.ds(0, 7), pl.ds(0, 768), :], g_snd.at[0])
+    whole(xs.at[0, pl.ds(0, 3)], g_snd.at[1])
     whole(xs.at[0, pl.ds(0, 7)], r_snd)
     whole(conv_all.at[pl.ds(0, 7)], p_snd)
     whole(sums_in, s_snd)
@@ -681,12 +722,15 @@
         scratch_shapes=[V(shape, dtype) for shape, dtype in RESULTS] + [
             V((TOK, SL), BF16),
             V((TOK, SL), BF16),
+            V((TOK, SL), BF16),
+            V((TOK, SL), BF16),
             V((2, TOK), jnp.int32),
             V((2, TOK), F32),
             V((N_TP, SL, SL), BF16),
             V((N_TP, SL, SL), BF16),
             V((N_TP, SL, SL), BF16),
             V((N_SP, 2, CAP, SL), BF16),
+            V((len(SECOND), 2, CAP, SL), BF16),
             V((2, N_TP, N_SP * CAP, SL), BF16),
             V((TOK, N_SP * CAP), BF16),
             V((NC, 2, NY, MAX, SL), BF16),
@@ -715,16 +759,16 @@
             V((8, TOK), F32),
             V((N_TP - 1, 8, TOK), F32),
             V((CH, TOK + 128), F32),
-            V((N_SP, CW // N_SP, SL), BF16),
-            V((N_SP, CW // N_SP, SL), BF16),
-            V((2, CW // N_SP, 128), F32),
-            V((NX, CW // N_SP, 128), F32),
+            V((N_TP, NX, CH // 2, 128), BF16),
+            V((N_SP, CH // 2, 128), BF16),
+            V((CH // 2, 128), F32),
+            V((CH // 2, 128), F32),
             pltpu.SemaphoreType.REGULAR((3,)),
-            D((12,)),
+            D((14,)),
             D((7,)),
-            D,
+            D((2,)),
             D((NC,)),
-            D,
+            D((2,)),
             D((NC, 7)),
             D,
             D((NC, 7)),
@@ -744,8 +788,8 @@
             D,
             D,
             D,
-            D((NX,)),
-            D((NX,)),
+            D,
+            D,
         ],
         compiler_params=pltpu.CompilerParams(
             collective_id=0, has_side_effects=True, vmem_limit_bytes=54 * 1024 * 1024

time: 104 us -> 94.9 us (0.913)
  Pallas kernels: 103 us -> 93.3 us
    pallas_call x1, Pallas kernels: 100 us -> 90.4 us  [main_call(): pl.pallas_call(main_kernel, out_shape=tuple((V(shape, dtype) for shape, d...]
where the time goes in v4:
time: 94.9 us; the launch traced here: 94.1 us
  Pallas kernels  93.3 us (98%)
    pallas_call x1, Pallas kernels, main_call(): pl.pallas_call(main_kernel, out_shape=tuple((V(shape, dtype) for shape, d...  90.4 us
    pallas_call x1, Pallas kernels, store_call(): pl.pallas_call(store_kernel, out_shape=tuple((jax.ShapeDtypeStruct(shape,...  2.84 us

profile of v4, /device:TPU:1, one launch (start us, length us, event | category | flops | bytes accessed | tf_op | source)
XLA Modules:
  0.0 94.1 jit_solution(1701561789206260656)
XLA Ops:
  0.6 90.4 %routed_experts.1 = (bf16[256,256]{1,0:T(8,128)(2,1)S(1)}, bf16[64,256]{1,0:T(8,128)(2,1)S(1)}, bf16[64,256]{1,0:T(8,128)(2,1)S(1)}, f32[64,64]{1,0:T(8,128)S(1)...) custom-call(bf16[256,2048]{1,0:T(8,128)(2,1)} %up_hbm.1, ...), custom_call_target="tpu_custom_call" | custom-call | flops 8589934592 | bytes 16777216 | tf_op jit(solution)/shard_map/routed_experts/pallas_call | solution.py:717
  91.1 2.8 %store_results.1 = (bf16[256,256]{1,0:T(8,128)(2,1)}, bf16[64,256]{1,0:T(8,128)(2,1)}, bf16[64,256]{1,0:T(8,128)(2,1)}, f32[64,64]{1,0:T(8,128)}, f32[8,256,256]...) custom-call(bf16[256,256]{1,0:T(8,128)(2,1)S(1)} %get-tuple-element.21.refs_0_, ...), custom_call_target="tpu_custom_call" | custom-call | tf_op jit(solution)/shard_map/store_results/pallas_call | solution.py:701

commit v5 on v4

--- a/solution.py
+++ b/solution.py
@@ -31,7 +31,7 @@
     + ((4, 0), (4, 1), (4, 2), (4, 3), (1, 2), (7, 2), (2, 2), (6, 2))
     + ((2, 1), (6, 1), (2, 3), (6, 3))
 )
-DIRECT = (0, 4)
+DIRECT = (0, 3, 4)
 SECOND = {p: i for i, p in enumerate(p for k in DIRECT for p in range(CHUNKS[k][0], sum(CHUNKS[k])))}
 OWN = 0
 
@@ -41,7 +41,7 @@
     return sorted(positions, key=lambda p: (-hops(p), p))
 
 
-G_SLOT = (0, 1, 6, 2, 3, 6, 4, 5, 6, 6, 6, 6, 6, 6)
+G_SLOT = (0, 1, 3, 1, 0, 3, 2, 2, 3, 3, 3, 3, 3, 3)
 CH = 64
 KW = 31
 
@@ -67,7 +67,7 @@
     row_out, ret, ggp, gup, act,
     value_v, gate_v, taps_v, conv_all, proj_all, hh, hn, mix, stat,
     pm, pm_in, pm_out, pm_got, sums, sums_in, conv_grad, gt, gt_in, gt_out, gt_got,
-    far_sem, load_sem, out_sem, a_snd, a_rcv, g_snd, g_rcv, r_snd, r_rcv, b_snd, b_rcv,
+    far_sem, load_sem, out_sem, a_snd, a_rcv, ao_rcv, g_snd, g_rcv, r_snd, r_rcv, b_snd, b_rcv,
     e_snd, e_rcv, j_snd, j_rcv, k_snd, k_rcv, p_snd, p_rcv, s_snd, s_rcv, h_snd, h_rcv, o_snd, o_rcv, f_snd, f_rcv,
 ):
     sp = lax.axis_index("sp")
@@ -175,7 +175,7 @@
             src_ref=send_o.at[SECOND[p]],
             dst_ref=xs.at[:, opp, pl.ds(p * CAP, CAP), :],
             send_sem=a_snd.at[1],
-            recv_sem=a_rcv.at[chunk_of[p]],
+            recv_sem=ao_rcv.at[chunk_of[p]],
             device_id=sp_dev(p, 1),
             device_id_type=MESH,
         )
@@ -233,8 +233,11 @@
                 xs[:, opp, pl.ds(p * CAP, CAP), :] = send_o[SECOND[p]]
             else:
                 a2a(p).start()
-                if k in DIRECT:
-                    a2a_o(p).start()
+
+    def stage_ox(k):
+        start, count = CHUNKS[k]
+        for p in range(max(start, 1), start + count):
+            a2a_o(p).start()
 
     def farther(step):
         for dev in (above, below):
@@ -250,6 +253,7 @@
     pl.semaphore_wait(barrier, len(near) + N_TP - 1)
     farther(0)
     stage_go(0)
+    stage_ox(0)
     for kind in range(4):
         conv_copy(kind).start()
     for r in range(1, N_TP):
@@ -258,7 +262,11 @@
     stage_go(1)
     stage_s(2)
     stage_f(1)
-    stage_go(2)
+
+    @pl.when(c == 0)
+    def _():
+        stage_go(2)
+
 
     def gather(k, kind, rc, slice_at, dev):
         start, count = CHUNKS[k]
@@ -280,44 +288,43 @@
         rc, slice_at, dev = plan[kind]
         return gather(k, kind, rc, slice_at, dev)
 
-    arrives = (bwd, fwd, other, bwd, fwd, other, opp, opp, bwd_o, fwd_o, opp_o, fwd_o, bwd_o, opp_o)
-    arrives_rc = (0, 0, 0, 1, 1, 1, 0, 1, 0, 0, 0, 1, 1, 1)
-
-    def got(k, kind):
-        gather(k, kind, arrives_rc[kind], arrives[kind], mate).wait_recv()
+    def both(k, slot):
+        start, count = CHUNKS[k]
+        whole(xs.at[:, tp, pl.ds(start * CAP, count * CAP), :], g_rcv.at[k, slot])
 
     def stage_a(k):
         start, count = CHUNKS[k]
         begin = max(start, 1)
-        slices = 2 if k in DIRECT else 1
-        whole(xs.at[:, pl.ds(0, slices), pl.ds(begin * CAP, (start + count - begin) * CAP), :], a_rcv.at[k])
-        for kind in (0, 4, 3, 1, 2, 5) + ((10, 13) if k in DIRECT else ()):
+        whole(xs.at[:, tp, pl.ds(begin * CAP, (start + count - begin) * CAP), :], a_rcv.at[k])
+        for kind in (0, 4, 3, 1, 2, 5):
             spread(k, kind).start()
 
+    def opposite(k):
+        start, count = CHUNKS[k]
+        begin = max(start, 1)
+        whole(xs.at[:, opp, pl.ds(begin * CAP, (start + count - begin) * CAP), :], ao_rcv.at[k])
+        spread(k, 10).start()
+        spread(k, 13).start()
+
     def stage_b1(k):
-        got(k, 0)
-        if k not in DIRECT:
-            spread(k, 6).start()
-        got(k, 4)
-        if k not in DIRECT:
-            spread(k, 7).start()
-        spread(k, 8).start()
-        spread(k, 11).start()
+        both(k, 0)
+        for kind in (8, 11) if k in DIRECT else (6, 7, 8, 11):
+            spread(k, kind).start()
 
     def stage_b2(k):
-        got(k, 1)
+        both(k, 1)
         spread(k, 9).start()
-        got(k, 3)
         spread(k, 12).start()
-        if k not in DIRECT:
-            got(k, 6)
+        if k in DIRECT:
+            opposite(k)
+        else:
+            both(k, 2)
             spread(k, 10).start()
-            got(k, 7)
             spread(k, 13).start()
 
     def stage_b3(k):
         start, count = CHUNKS[k]
-        whole(xs.at[:, pl.ds(0, NY), pl.ds(start * CAP, count * CAP), :], g_rcv.at[k, 6])
+        whole(xs.at[:, pl.ds(0, NY), pl.ds(start * CAP, count * CAP), :], g_rcv.at[k, 3])
 
     def swap(k):
         return pltpu.make_async_remote_copy(
@@ -475,8 +482,17 @@
     stage_f(2)
     stage_s(4)
     stage_a(1)
-    stage_go(3)
-    stage_go(4)
+
+    @pl.when(c == 0)
+    def _():
+        stage_go(3)
+        stage_go(4)
+        stage_ox(4)
+
+    @pl.when(c == 1)
+    def _():
+        stage_go(2)
+
     stage_b1(0)
     stage_b2(0)
     late[0].wait()
@@ -487,6 +503,13 @@
     stage_b1(1)
     stage_d(0)
     stage_a(2)
+
+    @pl.when(c == 1)
+    def _():
+        stage_go(3)
+        stage_go(4)
+        stage_ox(4)
+
     stage_m()
     stage_b2(1)
     stage_b3(1)
@@ -495,6 +518,7 @@
     stage_b1(2)
     stage_d(1)
     stage_a(3)
+    stage_ox(3)
     stage_e2(0)
     stage_n()
     stage_w(0, 384)
@@ -549,10 +573,14 @@
         odd = jnp.where(low_half, pltpu.roll(upper, CH, 1), lower)
         gt[:, 2 * g] = even.astype(BF16).reshape(N_TP, CH // 2, 128)
         gt[:, 2 * g + 1] = odd.astype(BF16).reshape(N_TP, CH // 2, 128)
+    def block_at(height):
+        ahead = (height - tp + NZ) % NZ
+        return 2 * ((y + ahead // 2 + 2) % NY) + ahead % 2
+
     def gt_copy(p):
         dev = sp_dev(p, 1)
         return pltpu.make_async_remote_copy(
-            src_ref=gt.at[dev[0] // NX, dev[0] % NX], dst_ref=gt_in.at[p], send_sem=o_snd, recv_sem=o_rcv,
+            src_ref=gt.at[block_at(dev[0] // NX), dev[0] % NX], dst_ref=gt_in.at[p], send_sem=o_snd, recv_sem=o_rcv,
             device_id=dev, device_id_type=MESH,
         )
 
@@ -612,24 +640,16 @@
     halo.start()
 
     whole(gt_in.at[pl.ds(1, N_SP - 1)], o_rcv)
-    owned = gt[z, x].astype(F32)
+    owned = gt[block_at(z), x].astype(F32)
     for p in range(N_SP):
         if p != OWN:
             owned = owned + gt_in[p].astype(F32)
     gt_out[...] = owned
-    here = z == tp
     owner_copy = pltpu.make_async_remote_copy(
         src_ref=gt_out, dst_ref=gt_got, send_sem=f_snd, recv_sem=f_rcv,
-        device_id=(tp * NX + x, z), device_id_type=MESH,
+        device_id=(tp * NX + x, block_at(z)), device_id_type=MESH,
     )
-
-    @pl.when(here)
-    def _():
-        gt_got[...] = gt_out[...]
-
-    @pl.when(jnp.logical_not(here))
-    def _():
-        owner_copy.start()
+    owner_copy.start()
 
     halo.wait_recv()
     tail = conv_grad[:, TOK:TOK + 128]
@@ -642,11 +662,8 @@
     gv_ref[...] = (glu * gate_sig).astype(BF16)
     gq_ref[...] = (glu * value_v[...].astype(F32) * gate_sig * (1.0 - gate_sig)).astype(BF16)
 
-    @pl.when(jnp.logical_not(here))
-    def _():
-        owner_copy.wait_recv()
-        owner_copy.wait_send()
-
+    owner_copy.wait_recv()
+    owner_copy.wait_send()
     got_t = gt_got[...].T
     go_ref[:, 0:CH // 2] = got_t[0:CH]
     go_ref[:, CH // 2:CH] = got_t[CH:2 * CH]
@@ -663,8 +680,8 @@
     whole(row_out.at[pl.ds(1, N_SP - 1)], b_snd)
     whole(gt_in.at[pl.ds(1, N_SP - 1)], o_snd)
 
-    whole(xs.at[:, pl.ds(0, 7), pl.ds(0, 768), :], g_snd.at[0])
-    whole(xs.at[0, pl.ds(0, 3)], g_snd.at[1])
+    whole(xs.at[:, pl.ds(0, 7), pl.ds(0, 512), :], g_snd.at[0])
+    whole(xs.at[:, pl.ds(0, 6), pl.ds(0, 512), :], g_snd.at[1])
     whole(xs.at[0, pl.ds(0, 7)], r_snd)
     whole(conv_all.at[pl.ds(0, 7)], p_snd)
     whole(sums_in, s_snd)
@@ -768,10 +785,11 @@
             D((7,)),
             D((2,)),
             D((NC,)),
+            D((NC,)),
             D((2,)),
-            D((NC, 7)),
-            D,
-            D((NC, 7)),
+            D((NC, 4)),
+            D,
+            D((NC, 4)),
             D,
             D((NC,)),
             D,

time: 94.9 us -> 91.1 us (0.960)
  Pallas kernels: 93.3 us -> 90.2 us
    pallas_call x1, Pallas kernels: 90.4 us -> 87.3 us  [main_call(): pl.pallas_call(main_kernel, out_shape=tuple((V(shape, dtype) for shape, d...]
where the time goes in v5:
time: 91.1 us; the launch traced here: 91 us
  Pallas kernels  90.2 us (99%)
    pallas_call x1, Pallas kernels, main_call(): pl.pallas_call(main_kernel, out_shape=tuple((V(shape, dtype) for shape, d...  87.3 us
    pallas_call x1, Pallas kernels, store_call(): pl.pallas_call(store_kernel, out_shape=tuple((jax.ShapeDtypeStruct(shape,...  2.84 us

profile of v5, /device:TPU:1, one launch (start us, length us, event | category | flops | bytes accessed | tf_op | source)
XLA Modules:
  0.0 91.0 jit_solution(11344207496169342566)
XLA Ops:
  0.6 87.3 %routed_experts.1 = (bf16[256,256]{1,0:T(8,128)(2,1)S(1)}, bf16[64,256]{1,0:T(8,128)(2,1)S(1)}, bf16[64,256]{1,0:T(8,128)(2,1)S(1)}, f32[64,64]{1,0:T(8,128)S(1)...) custom-call(bf16[256,2048]{1,0:T(8,128)(2,1)} %up_hbm.1, ...), custom_call_target="tpu_custom_call" | custom-call | flops 8589934592 | bytes 16777216 | tf_op jit(solution)/shard_map/routed_experts/pallas_call | solution.py:734
  88.0 2.8 %store_results.1 = (bf16[256,256]{1,0:T(8,128)(2,1)}, bf16[64,256]{1,0:T(8,128)(2,1)}, bf16[64,256]{1,0:T(8,128)(2,1)}, f32[64,64]{1,0:T(8,128)}, f32[8,256,256]...) custom-call(bf16[256,256]{1,0:T(8,128)(2,1)S(1)} %get-tuple-element.21.refs_0_, ...), custom_call_target="tpu_custom_call" | custom-call | tf_op jit(solution)/shard_map/store_results/pallas_call | solution.py:718

commit v6 on v5

--- a/solution.py
+++ b/solution.py
@@ -27,8 +27,8 @@
 OFFSETS = (
     ((0, 0), (1, 0), (7, 0), (0, 1))
     + ((0, 3), (0, 2), (1, 1), (7, 1), (1, 3), (7, 3), (2, 0), (6, 0))
+    + ((4, 0), (4, 1), (4, 2), (4, 3), (1, 2), (7, 2), (2, 2), (6, 2))
     + ((3, 0), (5, 0), (3, 1), (5, 1), (3, 2), (5, 2), (3, 3), (5, 3))
-    + ((4, 0), (4, 1), (4, 2), (4, 3), (1, 2), (7, 2), (2, 2), (6, 2))
     + ((2, 1), (6, 1), (2, 3), (6, 3))
 )
 DIRECT = (0, 3, 4)
@@ -262,6 +262,7 @@
     stage_go(1)
     stage_s(2)
     stage_f(1)
+    stage_f(2)
 
     @pl.when(c == 0)
     def _():
@@ -405,6 +406,37 @@
             return ring(k, 5, relay.at[k, 0, lo, :], 4, down_dev)
         return ring(k, 6, relay.at[k, 1, lo, :], 5, up_dev)
 
+    def straight(k, r):
+        size = CHUNKS[k][1] * CAP
+        return pltpu.make_async_remote_copy(
+            src_ref=comb.at[k, r, pl.ds(0, size), :], dst_ref=ring_in.at[k, r - 1, pl.ds(0, size), :],
+            send_sem=r_snd, recv_sem=r_rcv.at[k, 3],
+            device_id=(sp, ((y + r) % NY) * 2 + c), device_id_type=MESH,
+        )
+
+    def stage_last():
+        k = NC - 1
+        size = CHUNKS[k][1] * CAP
+        swap(k).wait_recv()
+        for r in (2, 1, 3, 0):
+            at = (y + r) % NY
+            pair = part[k, c, at, 0:size].astype(F32) + part_in[k, at, 0:size].astype(F32)
+            comb[k, r, 0:size] = pair.astype(BF16)
+            if r > 0:
+                straight(k, r).start()
+
+    def stage_end():
+        k = NC - 1
+        at, count = CHUNKS[k]
+        size = count * CAP
+        whole(ring_in.at[k, pl.ds(0, 3), pl.ds(0, size), :], r_rcv.at[k, 3])
+        total = comb[k, 0, 0:size].astype(F32)
+        for r in range(1, NY):
+            total = total + ring_in[k, r - 1, 0:size].astype(F32)
+        row_out[at:at + count] = total.astype(BF16).reshape(count, CAP, SL)
+        for p in far_first(range(at, at + count)):
+            back_copy(p).start()
+
     def stage_d(k):
         rings(k, 0).wait_recv()
         size = CHUNKS[k][1] * CAP
@@ -479,7 +511,6 @@
 
     stage_a(0)
     stage_s(3)
-    stage_f(2)
     stage_s(4)
     stage_a(1)
 
@@ -542,11 +573,10 @@
     stage_c(4)
     stage_e2(2)
     stage_e1(3)
-    stage_d(4)
+    stage_last()
     stage_w(640, 896)
-    stage_e1(4)
     stage_e2(3)
-    stage_e2(4)
+    stage_end()
     stage_w(896, 1024)
     outs = [
         pltpu.make_async_copy(acc_g, gg_out, out_sem.at[4]),

time: 91.1 us -> 90.7 us (level)
  no operation moved by 1% of the time
where the time goes in v6:
time: 90.7 us; the launch traced here: 90.6 us
  Pallas kernels  89.8 us (99%)
    pallas_call x1, Pallas kernels, main_call(): pl.pallas_call(main_kernel, out_shape=tuple((V(shape, dtype) for shape, d...  87 us
    pallas_call x1, Pallas kernels, store_call(): pl.pallas_call(store_kernel, out_shape=tuple((jax.ShapeDtypeStruct(shape,...  2.84 us

profile of v6, /device:TPU:1, one launch (start us, length us, event | category | flops | bytes accessed | tf_op | source)
XLA Modules:
  0.0 90.6 jit_solution(15355314069369191298)
XLA Ops:
  0.6 87.0 %routed_experts.1 = (bf16[256,256]{1,0:T(8,128)(2,1)S(1)}, bf16[64,256]{1,0:T(8,128)(2,1)S(1)}, bf16[64,256]{1,0:T(8,128)(2,1)S(1)}, f32[64,64]{1,0:T(8,128)S(1)...) custom-call(bf16[256,2048]{1,0:T(8,128)(2,1)} %up_hbm.1, ...), custom_call_target="tpu_custom_call" | custom-call | flops 8589934592 | bytes 16777216 | tf_op jit(solution)/shard_map/routed_experts/pallas_call | solution.py:764
  87.6 2.8 %store_results.1 = (bf16[256,256]{1,0:T(8,128)(2,1)}, bf16[64,256]{1,0:T(8,128)(2,1)}, bf16[64,256]{1,0:T(8,128)(2,1)}, f32[64,64]{1,0:T(8,128)}, f32[8,256,256]...) custom-call(bf16[256,256]{1,0:T(8,128)(2,1)S(1)} %get-tuple-element.21.refs_0_, ...), custom_call_target="tpu_custom_call" | custom-call | tf_op jit(solution)/shard_map/store_results/pallas_call | solution.py:748

commit v7 on v6

--- a/solution.py
+++ b/solution.py
@@ -261,14 +261,6 @@
     stage_f(0)
     stage_go(1)
     stage_s(2)
-    stage_f(1)
-    stage_f(2)
-
-    @pl.when(c == 0)
-    def _():
-        stage_go(2)
-
-
     def gather(k, kind, rc, slice_at, dev):
         start, count = CHUNKS[k]
         ref = xs.at[rc, slice_at, pl.ds(start * CAP, count * CAP), :]
@@ -509,7 +501,14 @@
             hh[k] = slope
             hn[k] = slope * n
 
+    stage_f(1)
     stage_a(0)
+    stage_f(2)
+
+    @pl.when(c == 0)
+    def _():
+        stage_go(2)
+
     stage_s(3)
     stage_s(4)
     stage_a(1)
@@ -550,13 +549,13 @@
     stage_d(1)
     stage_a(3)
     stage_ox(3)
-    stage_e2(0)
     stage_n()
     stage_w(0, 384)
     stage_b2(2)
     stage_b3(2)
     stage_c(2)
     stage_e1(1)
+    stage_e2(0)
     stage_b1(3)
     stage_d(2)
     stage_a(4)

time: 90.7 us -> 90.7 us (level)
  no operation moved by 1% of the time
where the time goes in v7:
time: 90.7 us; the launch traced here: 90.6 us
  Pallas kernels  89.8 us (99%)
    pallas_call x1, Pallas kernels, main_call(): pl.pallas_call(main_kernel, out_shape=tuple((V(shape, dtype) for shape, d...  86.9 us
    pallas_call x1, Pallas kernels, store_call(): pl.pallas_call(store_kernel, out_shape=tuple((jax.ShapeDtypeStruct(shape,...  2.84 us

profile of v7, /device:TPU:1, one launch (start us, length us, event | category | flops | bytes accessed | tf_op | source)
XLA Modules:
  0.0 90.6 jit_solution(12037183169059405120)
XLA Ops:
  0.6 86.9 %routed_experts.1 = (bf16[256,256]{1,0:T(8,128)(2,1)S(1)}, bf16[64,256]{1,0:T(8,128)(2,1)S(1)}, bf16[64,256]{1,0:T(8,128)(2,1)S(1)}, f32[64,64]{1,0:T(8,128)S(1)...) custom-call(bf16[256,2048]{1,0:T(8,128)(2,1)} %up_hbm.1, ...), custom_call_target="tpu_custom_call" | custom-call | flops 8589934592 | bytes 16777216 | tf_op jit(solution)/shard_map/routed_experts/pallas_call | solution.py:763
  87.6 2.8 %store_results.1 = (bf16[256,256]{1,0:T(8,128)(2,1)}, bf16[64,256]{1,0:T(8,128)(2,1)}, bf16[64,256]{1,0:T(8,128)(2,1)}, f32[64,64]{1,0:T(8,128)}, f32[8,256,256]...) custom-call(bf16[256,256]{1,0:T(8,128)(2,1)S(1)} %get-tuple-element.21.refs_0_, ...), custom_call_target="tpu_custom_call" | custom-call | tf_op jit(solution)/shard_map/store_results/pallas_call | solution.py:747
